TPU v7x, 256 devices: a 4x2x16 block of a 4x16x16 slice. The times are simulated.
256 devices in a mesh: grp: 2 (over y), sp: 32 (over z, core), tp: 4 (over x).
Axes of the slice: x: 4, y: 2, z: 16, core: 2. Of those that a mesh axis runs over, the one named last changes fastest.
The devices are a block of a 4x16x16 slice.
Arguments:
- resid: bfloat16 [40960, 2048], P(('grp', 'sp'), 'tp'), parts along dimension 0, may hold values from -6 to 6
- queries: bfloat16 [40960, 2048], P(('grp', 'sp'), 'tp'), parts along dimension 0, may hold values from -150 to 150
- keys_values: bfloat16 [40960, 8, 128], P(('grp', 'sp'), 'tp'), parts along dimension 0, may hold values from -4.5 to 4.5
- sink: float32 [32], P('tp'), may hold values from 3 to 7
- out_weight: bfloat16 [2048, 2048], P('tp'), may hold values from -2.390625 to 2.390625
- norm_gain: float32 [2048], replicated, may hold values from 0.1 to 1.9
- gate_weight: bfloat16 [2048, 5632], P('sp', 'tp'), may hold values from -0.125 to 0.125
- up_weight: bfloat16 [2048, 5632], P('sp', 'tp'), may hold values from -0.125 to 0.125
- down_weight: bfloat16 [5632, 2048], P('tp', 'sp'), may hold values from -0.078125 to 0.078125
Outputs:
- mixed: bfloat16 [40960, 2048], P(('grp', 'sp'), 'tp'), parts along dimension 0
There are 2 independent parts, one for each index of `grp`. A program takes and returns all parts, laid end to end along the dimension named above; an argument that names none is the same for every part. Nothing has to cross between parts.
All inputs are finite; a program needn't handle non-finite values.
Results may differ from a plain program's by a relative error of at most 0.008.
Values may be sent and summed in bfloat16 or wider, within the bound.
No kernel may reach another device: no remote copies, remote signals or barrier semaphores. Data moves between devices by JAX's collectives and lax.ppermute only.
A program may use at most 128 MiB of HBM per device.

v0:
```python
import jax
import jax.numpy as jnp
from jax import lax
from jax.sharding import PartitionSpec as P

HEAD_DIM = 64
WINDOW = 128
GRID_W = 64


def with_halo(cells, sides, width):
    for axis, dim in sides:
        count = lax.axis_size(axis)
        ends = count - 1
        head = lax.slice_in_dim(cells, 0, width, axis=dim)
        tail = lax.slice_in_dim(cells, cells.shape[dim] - width, cells.shape[dim], axis=dim)
        cells = jnp.concatenate(
            [
                lax.ppermute(tail, axis, [(i, (i + 1) % count) for i in range(ends)]),
                cells,
                lax.ppermute(head, axis, [((i + 1) % count, i) for i in range(ends)]),
            ],
            axis=dim,
        )
    return cells


def cut_along(array, dim, devices):
    before, after = (array.shape[:dim], array.shape[dim + 1 :])
    return jnp.moveaxis(array.reshape(*before, devices, -1, *after), dim, 0)


def sum_at_owner(array, axis, dim):
    blocks = cut_along(array, dim, lax.axis_size(axis))
    arrived = lax.all_to_all(blocks, axis, split_axis=0, concat_axis=0, tiled=True)
    return arrived.sum(axis=0)


def in_order(blocks, dim):
    shape = list(blocks.shape[1:])
    shape[dim] *= blocks.shape[0]
    return jnp.moveaxis(blocks, 0, dim).reshape(shape)


def copy_for_each(array, axis):
    copies = jnp.broadcast_to(array, (lax.axis_size(axis), *array.shape))
    return lax.all_to_all(copies, axis, split_axis=0, concat_axis=0, tiled=True)


def collect(array, axis, dim):
    return in_order(copy_for_each(array, axis), dim)


def side_by_side(arrays, axis, dim, along):
    both = jnp.concatenate(arrays, axis=along)
    out, at, done = (lax.all_gather(both, axis, axis=dim, tiled=True), 0, [])
    for a in arrays:
        done.append(lax.slice_in_dim(out, at, at + a.shape[along], axis=along))
        at += a.shape[along]
    return tuple(done)


def summed_on_arrival(array, axis, dim):
    blocks = cut_along(array, dim, lax.axis_size(axis))
    arrived = lax.all_to_all(blocks, axis, split_axis=0, concat_axis=0, tiled=True)
    return arrived.astype(jnp.float32).sum(axis=0)


def rotate(values, positions):
    quarter = 16
    inverse = 10000.0 ** (-jnp.arange(quarter, dtype=jnp.float32) / quarter)

    def turn(part, place):
        angle = place.astype(jnp.float32)[:, None] * inverse[None, :]
        cosine = jnp.cos(angle)[:, None, :]
        sine = jnp.sin(angle)[:, None, :]
        first, second = (part[..., :quarter], part[..., quarter:])
        return jnp.concatenate(
            [first * cosine - second * sine, second * cosine + first * sine], axis=-1
        )

    grid_row = positions // GRID_W
    grid_col = positions % GRID_W
    return jnp.concatenate(
        [turn(values[..., :32], grid_row), turn(values[..., 32:], grid_col)], axis=-1
    )


def body(
    resid, queries, keys_values, sink, out_weight, norm_gain, gate_weight, up_weight, down_weight
):
    tok = queries.shape[0]
    heads_here = queries.shape[1] // HEAD_DIM
    kv_here = keys_values.shape[1]
    group = heads_here // kv_here
    offset = lax.axis_index("sp") * tok
    total_tokens = tok * lax.axis_size("sp")
    positions = offset + jnp.arange(tok, dtype=jnp.int32)
    rotated_q = rotate(
        queries.astype(jnp.float32).reshape(tok, heads_here, HEAD_DIM), positions
    ).astype(jnp.bfloat16)
    rotated_k = rotate(keys_values[..., :HEAD_DIM].astype(jnp.float32), positions).astype(
        jnp.bfloat16
    )
    joined = jnp.concatenate([rotated_k, keys_values[..., HEAD_DIM:]], axis=-1)
    padded = with_halo(joined, (("sp", 0),), WINDOW)
    blocks = tok // WINDOW
    key_blocks = jnp.stack(
        [padded[index * WINDOW : index * WINDOW + 3 * WINDOW] for index in range(blocks)]
    )
    grouped = rotated_q.reshape(blocks, WINDOW, kv_here, group, HEAD_DIM)
    scores = jnp.einsum(
        "nqkgd,njkd->nkgqj", grouped, key_blocks[..., :HEAD_DIM], preferred_element_type=jnp.float32
    ) * HEAD_DIM ** (-0.5)
    block_start = offset + WINDOW * jnp.arange(blocks, dtype=jnp.int32)
    query_pos = block_start[:, None] + jnp.arange(WINDOW, dtype=jnp.int32)[None, :]
    key_pos = block_start[:, None] - WINDOW + jnp.arange(3 * WINDOW, dtype=jnp.int32)[None, :]
    valid = (
        (jnp.abs(query_pos[:, :, None] - key_pos[:, None, :]) <= WINDOW)
        & (key_pos[:, None, :] >= 0)
        & (key_pos[:, None, :] < total_tokens)
    )
    scores = jnp.where(valid[:, None, None], scores, jnp.float32(-1e30))
    sink_grid = sink.reshape(kv_here, group)[None, :, :, None]
    top = jnp.maximum(jnp.max(scores, axis=-1), sink_grid)
    expo = jnp.exp(scores - top[..., None])
    denom = jnp.sum(expo, axis=-1) + jnp.exp(sink_grid - top)
    probs = (expo / denom[..., None]).astype(jnp.bfloat16)
    attended = jnp.einsum(
        "nkgqj,njkd->nqkgd", probs, key_blocks[..., HEAD_DIM:], preferred_element_type=jnp.float32
    )
    attended = attended.astype(jnp.bfloat16).reshape(tok, heads_here * HEAD_DIM)
    partial_proj = jnp.dot(attended, out_weight, preferred_element_type=jnp.float32)
    projected = sum_at_owner(partial_proj, "tp", 1)
    stream_cols = (resid.astype(jnp.float32) + projected).astype(jnp.bfloat16)
    stream = collect(stream_cols, "tp", 1)
    widened = stream.astype(jnp.float32)
    normed = (
        widened * lax.rsqrt(jnp.mean(widened * widened, axis=-1, keepdims=True) + 1e-06) * norm_gain
    ).astype(jnp.bfloat16)
    pieces = side_by_side((gate_weight, up_weight), "sp", 0, 1)
    gate = jnp.dot(normed, pieces[0], preferred_element_type=jnp.float32)
    up = jnp.dot(normed, pieces[1], preferred_element_type=jnp.float32)
    hidden = (jax.nn.silu(gate) * up).astype(jnp.bfloat16)
    terms = jnp.dot(
        hidden,
        lax.all_gather(down_weight, "sp", axis=1, tiled=True),
        preferred_element_type=jnp.float32,
    )
    summed = summed_on_arrival(terms.astype(jnp.bfloat16), "tp", 1)
    return (stream_cols.astype(jnp.float32) + summed).astype(jnp.bfloat16)


def solution(mesh):
    return jax.shard_map(
        body,
        mesh=mesh,
        in_specs=(
            P(("grp", "sp"), "tp"),
            P(("grp", "sp"), "tp"),
            P(("grp", "sp"), "tp", None),
            P("tp"),
            P("tp", None),
            P(),
            P("sp", "tp"),
            P("sp", "tp"),
            P("tp", "sp"),
        ),
        out_specs=P(("grp", "sp"), "tp"),
        check_vma=False,
    )
```

profile of v0, /device:TPU:33, one launch (start us, length us, event | category | flops | bytes accessed | tf_op | source)
XLA Modules:
  0.0 236.5 jit_solution(14854409233111886337)
XLA Ops:
  6.6 1.9 pad_maximum_fusion
  8.5 1.7 fusion.54
  11.2 0.7 fusion.53
  11.9 5.7 %collective-permute-start = (bf16[128,2,128]{0,2,1:T(8,128)(2,1)}, bf16[128,2,128]{0,2,1:T(8,128)(2,1)S(1)}, u32[]{:S(2)}, u32[]{:S(2)}) collective-permute-start(bf16[128,2,128]{0,2,1:T(8,128)(2,1)} %get-tuple-element.12), channel_id=1, source_target_pairs={{0,4},{4,8},{8,12},{12,16},{16,20},{20,24},{24,28},{28,32},{32,36}... | collective-permute-start | bytes 196616 | tf_op jit(solution)/shard_map/ppermute | solution.py:19
  17.6 17.9 %collective-permute-start.1 = (bf16[128,2,128]{0,2,1:T(8,128)(2,1)S(1)}, bf16[128,2,128]{0,2,1:T(8,128)(2,1)S(1)}, u32[]{:S(2)}, u32[]{:S(2)}) collective-permute-start(bf16[128,2,128]{0,2,1:T(8,128)(2,1)S(1)} %get-tuple-element.11), channel_id=1, source_target_pairs={{4,0},{8,4},{12,8},{16,12},{20,16},{24,20},{28,24},{32,28},{36,32}... | collective-permute-start | bytes 196616 | tf_op jit(solution)/shard_map/ppermute | solution.py:21
  36.4 1.2 fusion.18
  38.6 2.9 %copy.48 = bf16[2048,512]{1,0:T(8,128)(2,1)S(1)} copy(bf16[2048,512]{0,1:T(8,128)(2,1)} %bitcast.87) | data formatting | bytes 4194304 | tf_op jit(solution)/shard_map/dot_general | solution.py:133
  41.7 1.3 fusion.1
  43.1 1.9 fusion
  45.1 2.3 fusion.16
  47.5 0.5 copy.38
  47.9 1.6 reshape.277
  49.6 2.7 %convolution_bitcast_fusion = f32[4,640,512]{2,1,0:T(8,128)S(1)} fusion(bf16[640,512,1]{0,1,2:T(8,128)(2,1)} %reshape.277, bf16[4,512,512]{2,1,0:T(8,128)(2,1)S(1)} %bitcast.84), kind=kOutput, calls=%fused_computation.19 | convolution fusion | flops 1342177280 | bytes 7995392 | tf_op jit(solution)/shard_map/dot_general | solution.py:133
  52.2 63.9 %all_to_all.15 = f32[4,640,512]{2,1,0:T(8,128)} all-to-all(f32[4,640,512]{2,1,0:T(8,128)S(1)} %convolution_bitcast_fusion), channel_id=1, replica_groups=mesh['grp'=2,'sp'=32,'tp'=4] {'tp'}, dimensions={0} | all-to-all | bytes 10485760 | tf_op jit(solution)/shard_map/all_to_all | solution.py:35
  116.1 3.3 %reduce_sum.37 = f32[640,512]{1,0:T(8,128)S(1)} reduce(f32[4,640,512]{2,1,0:T(8,128)} %all_to_all.15, f32[]{:T(128)} %constant.67.clone.1), dimensions={0}, to_apply=%region_2.3 | reduce | flops 983040 | bytes 6553604 | tf_op jit(solution)/shard_map/reduce_sum | solution.py:36
  120.2 34.2 %all_to_all.16 = bf16[4,640,512]{1,2,0:T(8,128)(2,1)S(1)} all-to-all(bf16[4,640,512]{1,2,0:T(8,128)(2,1)S(1)} %broadcast_in_dim.12), channel_id=1, replica_groups=mesh['grp'=2,'sp'=32,'tp'=4] {'tp'}, dimensions={0} | all-to-all | bytes 5242880 | tf_op jit(solution)/shard_map/all_to_all | solution.py:47
  154.3 0.6 multiply_reduce_fusion
  155.0 0.6 fusion.7
  155.6 9.7 %fusion.4 = f32[640,1408]{1,0:T(8,128)} fusion(bf16[640,2048]{0,1:T(8,128)(2,1)S(1)} %fusion.7, bf16[2048,2816]{1,0:T(8,128)(2,1)} %all-gather.3.cloned.1.call-done), kind=kOutput, calls=%fused_computation.7 | convolution fusion | flops 3690987520 | bytes 11993088 | tf_op jit(solution)/shard_map/dot_general | solution.py:142
  165.3 12.4 %all-gather.5.cloned.1.call-done = bf16[1408,2048]{0,1:T(8,128)(2,1)} async-done(((bf16[1408,64]{0,1:T(8,128)(2,1)}), bf16[1408,2048]{0,1:T(8,128)(2,1)}) %all-gather.5.cloned.1.call-update) | async-done | bytes 5767184 | tf_op jit(solution)/shard_map/all_gather | solution.py:147
  177.7 14.8 %convolution_convert_fusion = bf16[640,2048]{1,0:T(8,128)(2,1)S(1)} fusion(bf16[1408,2048]{0,1:T(8,128)(2,1)} %all-gather.5.cloned.1.call-done, bf16[640,2048]{0,1:T(8,128)(2,1)} %copy-done, bf16[2048,2816]{1,0:T(8,128)(2,1)} %all-gather.3.cloned.1.call-done, f32[640,1408]{1,0:T(8,128)} %fusion.4), kind=kOutput, calls=%fused_computation.17 | convolution fusion | flops 7388692480 | bytes 20381696 | tf_op jit(solution)/shard_map/dot_general | solution.py:145
  192.8 35.3 %all_to_all.17 = bf16[4,640,512]{2,1,0:T(8,128)(2,1)S(1)} all-to-all(bf16[4,640,512]{2,1,0:T(8,128)(2,1)S(1)} %bitcast.83), channel_id=1, replica_groups=mesh['grp'=2,'sp'=32,'tp'=4] {'tp'}, dimensions={0} | all-to-all | bytes 5242880 | tf_op jit(solution)/shard_map/all_to_all | solution.py:65
  228.1 0.4 convert_reduce_fusion
  228.5 1.1 add_convert_fusion
  (56 shorter events, 4.1 us)
Async XLA Ops:
  6.5 29.2 %copy-start.2 = (bf16[640,512]{1,0:T(8,128)(2,1)S(1)}, bf16[640,512]{1,0:T(8,128)(2,1)}, u32[]{:S(2)}) copy-start(bf16[640,512]{1,0:T(8,128)(2,1)} %param.10) | copy-start | bytes 1966084
  6.5 149.1 %all-gather.3.cloned.1.call-start = ((), (), s32[]{:S(2)}) async-start(), calls=%async_computation.3 | async-start | bytes 11894784 | tf_op jit(solution)/shard_map/all_gather | solution.py:56
  8.5 169.3 %all-gather.5.cloned.1.call-start = ((), (), s32[]{:S(2)}) async-start(), calls=%async_computation.4 | async-start | bytes 5947392 | tf_op jit(solution)/shard_map/all_gather | solution.py:147
  11.9 29.6 %collective-permute-start = (bf16[128,2,128]{0,2,1:T(8,128)(2,1)}, bf16[128,2,128]{0,2,1:T(8,128)(2,1)S(1)}, u32[]{:S(2)}, u32[]{:S(2)}) collective-permute-start(bf16[128,2,128]{0,2,1:T(8,128)(2,1)} %get-tuple-element.12), channel_id=1, source_target_pairs={{0,4},{4,8},{8,12},{12,16},{16,20},{20,24},{24,28},{28,32},{32,36}... | collective-permute-start | bytes 196616 | tf_op jit(solution)/shard_map/ppermute | solution.py:19
  17.6 24.1 %collective-permute-start.1 = (bf16[128,2,128]{0,2,1:T(8,128)(2,1)S(1)}, bf16[128,2,128]{0,2,1:T(8,128)(2,1)S(1)}, u32[]{:S(2)}, u32[]{:S(2)}) collective-permute-start(bf16[128,2,128]{0,2,1:T(8,128)(2,1)S(1)} %get-tuple-element.11), channel_id=1, source_target_pairs={{4,0},{8,4},{12,8},{16,12},{20,16},{24,20},{28,24},{32,28},{36,32}... | collective-permute-start | bytes 196616 | tf_op jit(solution)/shard_map/ppermute | solution.py:21
  36.0 2.5 %copy-start.4 = (f32[8]{0:T(128)S(1)}, f32[8]{0:T(128)}, u32[]{:S(2)}) copy-start(f32[8]{0:T(128)} %param.12) | copy-start | bytes 100
  116.1 3.3 %copy-start.1 = (bf16[640,512]{1,0:T(8,128)(2,1)S(1)}, bf16[640,512]{1,0:T(8,128)(2,1)}, u32[]{:S(2)}) copy-start(bf16[640,512]{1,0:T(8,128)(2,1)} %param.9) | copy-start | bytes 1966084
  120.2 34.8 %copy-start.3 = (f32[2048]{0:T(1024)S(1)}, f32[2048]{0:T(1024)}, u32[]{:S(2)}) copy-start(f32[2048]{0:T(1024)} %param.14) | copy-start | bytes 24580
  155.6 9.7 %copy-start = (bf16[640,2048]{0,1:T(8,128)(2,1)}, bf16[640,2048]{0,1:T(8,128)(2,1)S(1)}, u32[]{:S(2)}) copy-start(bf16[640,2048]{0,1:T(8,128)(2,1)S(1)} %fusion.7) | copy-start | bytes 7864324
Sparse Core Ops, SparseCore 0:
  9.2 96.4 all-gather.2
  107.6 70.1 all-gather.4
where the time goes:
time: 237 us; the launch traced here: 236 us
  blocking collectives  133 us (56%)
  matrix products  30.8 us (13%)
  starting transfers between devices  23.7 us (10%)
  between operations  13.8 us (6%)
  waiting for transfers between devices  12.6 us (5%)
  other arithmetic  12.5 us (5%)
  local copies, waits for them, and re-layouts  9.78 us (4%)
    all_to_all x1, blocking collectives, sum_at_owner(): lax.all_to_all(blocks, axis, split_axis=0, concat_axis=0, tiled=True)  63.9 us
    all_to_all x1, blocking collectives, summed_on_arrival(): lax.all_to_all(blocks, axis, split_axis=0, concat_axis=0, tiled=True)  35.3 us
    all_to_all x1, blocking collectives, copy_for_each(): return lax.all_to_all(copies, axis, split_axis=0, concat_axis=0, tiled=True)  34.2 us
    ppermute x1, starting transfers between devices, with_halo(): lax.ppermute(head, axis, [((i + 1) % count, i) for i in range(ends)])  17.9 us
    dot_general x1, matrix products, body(): jnp.dot(hidden, lax.all_gather(down_weight, 'sp', axis=1, tiled=True), pr...  14.8 us
    all_gather x1, waiting for transfers between devices, body(): lax.all_gather(down_weight, 'sp', axis=1, tiled=True)  12.4 us
    dot_general x1, matrix products, body(): gate = jnp.dot(normed, pieces[0], preferred_element_type=jnp.float32)  9.66 us
    ppermute x1, starting transfers between devices, with_halo(): lax.ppermute(tail, axis, [(i, (i + 1) % count) for i in range(ends)])  5.73 us
  transfers between devices with their start and end apart: 4, of which 1 were waited for; matrix products, arithmetic and copies ran while one was open for 15% of the time, Pallas kernels for 0%

commit v1 on v0

--- a/solution.py
+++ b/solution.py
@@ -131,21 +131,19 @@
     )
     attended = attended.astype(jnp.bfloat16).reshape(tok, heads_here * HEAD_DIM)
     partial_proj = jnp.dot(attended, out_weight, preferred_element_type=jnp.float32)
-    projected = sum_at_owner(partial_proj, "tp", 1)
+    projected = summed_on_arrival(partial_proj.astype(jnp.bfloat16), "tp", 1)
     stream_cols = (resid.astype(jnp.float32) + projected).astype(jnp.bfloat16)
     stream = collect(stream_cols, "tp", 1)
     widened = stream.astype(jnp.float32)
     normed = (
         widened * lax.rsqrt(jnp.mean(widened * widened, axis=-1, keepdims=True) + 1e-06) * norm_gain
     ).astype(jnp.bfloat16)
-    pieces = side_by_side((gate_weight, up_weight), "sp", 0, 1)
+    pieces = side_by_side((gate_weight, up_weight, down_weight.T), "sp", 0, 1)
     gate = jnp.dot(normed, pieces[0], preferred_element_type=jnp.float32)
     up = jnp.dot(normed, pieces[1], preferred_element_type=jnp.float32)
-    hidden = (jax.nn.silu(gate) * up).astype(jnp.bfloat16)
-    terms = jnp.dot(
-        hidden,
-        lax.all_gather(down_weight, "sp", axis=1, tiled=True),
-        preferred_element_type=jnp.float32,
+    hidden = lax.optimization_barrier((jax.nn.silu(gate) * up).astype(jnp.bfloat16))
+    terms = lax.dot_general(
+        hidden, pieces[2], (((1,), (1,)), ((), ())), preferred_element_type=jnp.float32
     )
     summed = summed_on_arrival(terms.astype(jnp.bfloat16), "tp", 1)
     return (stream_cols.astype(jnp.float32) + summed).astype(jnp.bfloat16)

time: 237 us -> 195 us (0.82)
  blocking collectives: 133 us -> 104 us
  matrix products: 30.8 us -> 23.8 us
  waiting for transfers between devices: 12.6 us -> 5.63 us
    all_to_all x1 -> x0, blocking collectives: 63.9 us -> none  [sum_at_owner(): lax.all_to_all(blocks, axis, split_axis=0, concat_axis=0, tiled=True)]
    all_to_all x1 -> x2, blocking collectives: 35.3 us -> 70.3 us  [summed_on_arrival(): lax.all_to_all(blocks, axis, split_axis=0, concat_axis=0, tiled=True)]
    all_gather x1 -> x0, waiting for transfers between devices: 12.4 us -> none  [body(): lax.all_gather(down_weight, 'sp', axis=1, tiled=True)]
    all_gather x1, waiting for transfers between devices: 0.02 us -> 5.57 us  [side_by_side(): out, at, done = (lax.all_gather(both, axis, axis=dim, tiled=True), 0, [])]
    dot_general x1 -> x2, matrix products: 14.8 us -> 9.56 us  [the longest x1 5.04 us: body(): up = jnp.dot(normed, pieces[1], preferred_element_type=jnp.float32)]
    reduce_sum x1 -> x0, other arithmetic: 3.3 us -> none  [sum_at_owner(): return arrived.sum(axis=0)]
    concatenate x8, local copies, waits for them, and re-layouts: 0.89 us -> 3.8 us  [rotate(): jnp.concatenate([turn(values[..., :32], grid_row), turn(values[..., 32:],...]
    dot_general x1 -> x0, local copies, waits for them, and re-layouts: 2.86 us -> none  [body(): jnp.dot(attended, out_weight, preferred_element_type=jnp.float32)]
  transfers between devices with their start and end apart: 4 -> 3, of which waited for: 1 -> 1; matrix products, arithmetic and copies ran while one was open for 15% -> 13% of each run, Pallas kernels for 0% -> 0%
where the time goes in v1:
time: 195 us
  blocking collectives  104 us (53%)
  matrix products  23.8 us (12%)
  starting transfers between devices  23.6 us (12%)
  between operations  13.8 us (7%)
  other arithmetic  12 us (6%)
  local copies, waits for them, and re-layouts  11.6 us (6%)
  waiting for transfers between devices  5.63 us (3%)
    all_to_all x2, blocking collectives, summed_on_arrival(): lax.all_to_all(blocks, axis, split_axis=0, concat_axis=0, tiled=True)  70.3 us
    all_to_all x1, blocking collectives, copy_for_each(): return lax.all_to_all(copies, axis, split_axis=0, concat_axis=0, tiled=True)  34.2 us
    ppermute x1, starting transfers between devices, with_halo(): lax.ppermute(head, axis, [((i + 1) % count, i) for i in range(ends)])  17.9 us
    dot_general x1, matrix products, body(): gate = jnp.dot(normed, pieces[0], preferred_element_type=jnp.float32)  8.05 us
    ppermute x1, starting transfers between devices, with_halo(): lax.ppermute(tail, axis, [(i, (i + 1) % count) for i in range(ends)])  5.73 us
    all_gather x1, waiting for transfers between devices, side_by_side(): out, at, done = (lax.all_gather(both, axis, axis=dim, tiled=True), 0, [])  5.57 us
    dot_general x1, matrix products, body(): up = jnp.dot(normed, pieces[1], preferred_element_type=jnp.float32)  5.04 us
    dot_general x1, matrix products, body(): lax.dot_general(hidden, pieces[2], (((1,), (1,)), ((), ())), preferred_el...  4.51 us
  transfers between devices with their start and end apart: 3, of which 1 were waited for; matrix products, arithmetic and copies ran while one was open for 13% of the time, Pallas kernels for 0%

profile of v1, /device:TPU:33, one launch (start us, length us, event | category | flops | bytes accessed | tf_op | source)
XLA Modules:
  0.0 194.8 jit_solution(336408478782344842)
XLA Ops:
  6.6 2.1 %pad_maximum_fusion = bf16[64,4224]{1,0:T(8,128)(2,1)} fusion(bf16[64,1408]{1,0:T(8,128)(2,1)} %bitcast.97, bf16[64,1408]{1,0:T(8,128)(2,1)} %param.16, bf16[64,1408]{1,0:T(8,128)(2,1)} %param.15), kind=kLoop, calls=%fused_computation.41 | loop fusion | flops 1622016 | bytes 1081344 | tf_op jit(solution)/shard_map/concatenate | solution.py:55
  8.7 1.7 fusion.58
  12.0 5.7 %collective-permute-start = (bf16[128,2,128]{0,2,1:T(8,128)(2,1)}, bf16[128,2,128]{0,2,1:T(8,128)(2,1)S(1)}, u32[]{:S(2)}, u32[]{:S(2)}) collective-permute-start(bf16[128,2,128]{0,2,1:T(8,128)(2,1)} %get-tuple-element.12), channel_id=1, source_target_pairs={{0,4},{4,8},{8,12},{12,16},{16,20},{20,24},{24,28},{28,32},{32,36}... | collective-permute-start | bytes 196616 | tf_op jit(solution)/shard_map/ppermute | solution.py:19
  17.8 17.9 %collective-permute-start.1 = (bf16[128,2,128]{0,2,1:T(8,128)(2,1)}, bf16[128,2,128]{0,2,1:T(8,128)(2,1)S(1)}, u32[]{:S(2)}, u32[]{:S(2)}) collective-permute-start(bf16[128,2,128]{0,2,1:T(8,128)(2,1)} %get-tuple-element.11), channel_id=1, source_target_pairs={{4,0},{8,4},{12,8},{16,12},{20,16},{24,20},{28,24},{32,28},{36,32}... | collective-permute-start | bytes 196616 | tf_op jit(solution)/shard_map/ppermute | solution.py:21
  35.7 1.4 copy.29
  37.4 0.8 subtract_convert_fusion.1
  38.2 1.2 fusion.23
  39.4 1.1 concatenate.32
  41.4 0.7 copy.31
  43.2 0.7 max.17
  44.2 2.2 %fusion.1 = (f32[5,2,4,128]{3,2,1,0:T(4,128)S(1)}, f32[5,2,384,128,4]{3,2,4,1,0:T(8,128)S(1)}) fusion(pred[5,128,384]{1,2,0:T(8,128)(4,1)S(1)} %fusion.23, bf16[5,128,2,4,16]{1,4,3,2,0:T(8,128)(2,1)S(1)} %copy.33, bf16[5,128,2,4,16]{1,4,3,2,0:T(8,128)(2,1)} %copy.32, bf16[5,128,2,4,16]{1,4,3,2,0:T(8,128)(2,1)} %copy.31, ...), kind=kOutput, calls=%fused_computation.4 | convolution fusion | flops 260172800 | bytes 9277440 | tf_op jit(solution)/shard_map/nqkgd,njkd->nkgqj/dot_general | solution.py:112
  46.5 1.9 fusion
  48.5 2.3 %fusion.21 = bf16[5,128,2,4,64]{1,4,3,2,0:T(8,128)(2,1)S(1)} fusion(f32[5,2,384,128,4]{3,2,4,1,0:T(8,128)S(1)} %get-tuple-element.24, f32[5,2,4,128]{3,2,1,0:T(4,128)S(1)} %exponential_add_fusion, f32[5,2,4,128]{3,2,1,0:T(4,128)S(1)} %broadcast_maximum_fusion, pred[5,128,384]{1,2,0:T(8,128)(4,1)S(1)} %fusion.23, bf16[5,384,2,128]{1,3,2,0:T(8,128)(2,1)S(1)} %fusion.35), kind=kOutput, calls=%fused_computation.27 | convolution fusion | flops 261816320 | bytes 9297920 | tf_op jit(solution)/shard_map/nkgqj,njkd->nqkgd/dot_general | solution.py:129
  51.4 1.6 convolution_convert_fusion
  53.2 34.8 %all_to_all.15 = bf16[4,640,512]{2,1,0:T(8,128)(2,1)S(1)} all-to-all(bf16[4,640,512]{2,1,0:T(8,128)(2,1)S(1)} %bitcast.91), channel_id=1, replica_groups=mesh['grp'=2,'sp'=32,'tp'=4] {'tp'}, dimensions={0} | all-to-all | bytes 5242880 | tf_op jit(solution)/shard_map/all_to_all | solution.py:65
  89.2 34.2 %all_to_all.16 = bf16[4,640,512]{1,2,0:T(8,128)(2,1)S(1)} all-to-all(bf16[4,640,512]{1,2,0:T(8,128)(2,1)S(1)} %broadcast_in_dim.12), channel_id=1, replica_groups=mesh['grp'=2,'sp'=32,'tp'=4] {'tp'}, dimensions={0} | all-to-all | bytes 5242880 | tf_op jit(solution)/shard_map/all_to_all | solution.py:47
  124.0 2.2 %fusion.9 = bf16[640,2048]{0,1:T(8,128)(2,1)} fusion(f32[2048]{0:T(1024)S(1)} %copy-done.5, f32[640]{0:T(1024)S(1)} %add_rsqrt_fusion, bf16[4,640,512]{1,2,0:T(8,128)(2,1)S(1)} %all_to_all.16), kind=kLoop, calls=%fused_computation.13 | loop fusion | flops 5242880 | bytes 5253632 | tf_op jit(solution)/shard_map/convert_element_type | solution.py:140
  126.2 5.6 %all-gather.2.cloned.1.call-done = bf16[2048,4224]{1,0:T(8,128)(2,1)} async-done(((bf16[64,4224]{1,0:T(8,128)(2,1)}), bf16[2048,4224]{1,0:T(8,128)(2,1)}) %all-gather.2.cloned.1.call-update) | async-done | bytes 17301520 | tf_op jit(solution)/shard_map/all_gather | solution.py:56
  131.8 8.0 %fusion.6 = f32[640,1408]{1,0:T(8,128)S(1)} fusion(bf16[640,2048]{0,1:T(8,128)(2,1)} %fusion.9, bf16[2048,4224]{1,0:T(8,128)(2,1)} %all-gather.2.cloned.1.call-done), kind=kOutput, calls=%fused_computation.9 | convolution fusion | flops 3690987520 | bytes 11993088 | tf_op jit(solution)/shard_map/dot_general | solution.py:142
  139.8 1.3 copy-done.6
  141.1 5.0 %fusion.14 = bf16[640,1408]{1,0:T(8,128)(2,1)S(1)} fusion(bf16[640,2048]{0,1:T(8,128)(2,1)S(1)} %copy-done.2, bf16[2048,4224]{1,0:T(8,128)(2,1)S(1)} %copy-done.6, f32[640,1408]{1,0:T(8,128)S(1)} %fusion.6), kind=kOutput, calls=%fused_computation.19 | convolution fusion | flops 3696394240 | bytes 13795328 | tf_op jit(solution)/shard_map/dot_general | solution.py:143
  146.2 4.5 %fusion.17 = bf16[640,2048]{1,0:T(8,128)(2,1)S(1)} fusion(bf16[640,1408]{1,0:T(8,128)(2,1)S(1)} %fusion.14, bf16[2048,4224]{1,0:T(8,128)(2,1)S(1)} %copy-done.6), kind=kOutput, calls=%fused_computation.20 | convolution fusion | flops 3692298240 | bytes 10190848 | tf_op jit(solution)/shard_map/dot_general | solution.py:145
  150.9 35.5 %all_to_all.17 = bf16[4,640,512]{2,1,0:T(8,128)(2,1)S(1)} all-to-all(bf16[4,640,512]{2,1,0:T(8,128)(2,1)S(1)} %bitcast.92), channel_id=1, replica_groups=mesh['grp'=2,'sp'=32,'tp'=4] {'tp'}, dimensions={0} | all-to-all | bytes 5242880 | tf_op jit(solution)/shard_map/all_to_all | solution.py:65
  186.8 1.1 add_convert_fusion
  (57 shorter events, 7.5 us)
Async XLA Ops:
  6.5 44.8 %copy-start = (bf16[512,2048]{1,0:T(8,128)(2,1)S(1)}, bf16[512,2048]{1,0:T(8,128)(2,1)}, u32[]{:S(2)}) copy-start(bf16[512,2048]{1,0:T(8,128)(2,1)} %param.13) | copy-start | bytes 6291460
  6.6 125.2 %all-gather.2.cloned.1.call-start = ((), (), s32[]{:S(2)}) async-start(), calls=%async_computation.3 | async-start | bytes 17842176 | tf_op jit(solution)/shard_map/all_gather | solution.py:56
  12.0 31.9 %collective-permute-start = (bf16[128,2,128]{0,2,1:T(8,128)(2,1)}, bf16[128,2,128]{0,2,1:T(8,128)(2,1)S(1)}, u32[]{:S(2)}, u32[]{:S(2)}) collective-permute-start(bf16[128,2,128]{0,2,1:T(8,128)(2,1)} %get-tuple-element.12), channel_id=1, source_target_pairs={{0,4},{4,8},{8,12},{12,16},{16,20},{20,24},{24,28},{28,32},{32,36}... | collective-permute-start | bytes 196616 | tf_op jit(solution)/shard_map/ppermute | solution.py:19
  17.8 26.4 %collective-permute-start.1 = (bf16[128,2,128]{0,2,1:T(8,128)(2,1)}, bf16[128,2,128]{0,2,1:T(8,128)(2,1)S(1)}, u32[]{:S(2)}, u32[]{:S(2)}) collective-permute-start(bf16[128,2,128]{0,2,1:T(8,128)(2,1)} %get-tuple-element.11), channel_id=1, source_target_pairs={{4,0},{8,4},{12,8},{16,12},{20,16},{24,20},{28,24},{32,28},{36,32}... | collective-permute-start | bytes 196616 | tf_op jit(solution)/shard_map/ppermute | solution.py:21
  42.1 2.1 %copy-start.4 = (bf16[5,128,2,4,16]{1,4,3,2,0:T(8,128)(2,1)S(1)}, bf16[5,128,2,4,16]{1,4,3,2,0:T(8,128)(2,1)}, u32[]{:S(2)}) copy-start(bf16[5,128,2,4,16]{1,4,3,2,0:T(8,128)(2,1)} %copy.30) | copy-start | bytes 491524
  53.2 35.3 %copy-start.3 = (bf16[640,512]{1,0:T(8,128)(2,1)S(1)}, bf16[640,512]{1,0:T(8,128)(2,1)}, u32[]{:S(2)}) copy-start(bf16[640,512]{1,0:T(8,128)(2,1)} %param.9) | copy-start | bytes 1966084
  89.2 34.8 %copy-start.5 = (f32[2048]{0:T(1024)S(1)}, f32[2048]{0:T(1024)}, u32[]{:S(2)}) copy-start(f32[2048]{0:T(1024)} %param.14) | copy-start | bytes 24580
  131.8 8.1 %copy-start.2 = (bf16[640,2048]{0,1:T(8,128)(2,1)S(1)}, bf16[640,2048]{0,1:T(8,128)(2,1)}, u32[]{:S(2)}) copy-start(bf16[640,2048]{0,1:T(8,128)(2,1)} %fusion.9) | copy-start | bytes 7864324
  131.8 9.4 %copy-start.6 = (bf16[2048,4224]{1,0:T(8,128)(2,1)S(1)}, bf16[2048,4224]{1,0:T(8,128)(2,1)}, u32[]{:S(2)}) copy-start(bf16[2048,4224]{1,0:T(8,128)(2,1)} %all-gather.2.cloned.1.call-done) | copy-start | bytes 51904516
  150.9 37.0 %copy-start.1 = (bf16[512,2048]{1,0:T(8,128)(2,1)S(1)}, bf16[512,2048]{1,0:T(8,128)(2,1)}, u32[]{:S(2)}) copy-start(bf16[512,2048]{1,0:T(8,128)(2,1)} %param.13) | copy-start | bytes 6291460
Sparse Core Ops, SparseCore 0:
  9.2 122.5 all-gather.1

commit v2 on v1

--- a/solution.py
+++ b/solution.py
@@ -1,7 +1,10 @@
 import jax
 import jax.numpy as jnp
 from jax import lax
+from jax.experimental import pallas as pl
+from jax.experimental.pallas import tpu as pltpu
 from jax.sharding import PartitionSpec as P
+
 
 HEAD_DIM = 64
 WINDOW = 128
@@ -25,45 +28,347 @@
     return cells
 
 
-def cut_along(array, dim, devices):
-    before, after = (array.shape[:dim], array.shape[dim + 1 :])
-    return jnp.moveaxis(array.reshape(*before, devices, -1, *after), dim, 0)
-
-
-def sum_at_owner(array, axis, dim):
-    blocks = cut_along(array, dim, lax.axis_size(axis))
-    arrived = lax.all_to_all(blocks, axis, split_axis=0, concat_axis=0, tiled=True)
-    return arrived.sum(axis=0)
-
-
-def in_order(blocks, dim):
-    shape = list(blocks.shape[1:])
-    shape[dim] *= blocks.shape[0]
-    return jnp.moveaxis(blocks, 0, dim).reshape(shape)
-
-
-def copy_for_each(array, axis):
-    copies = jnp.broadcast_to(array, (lax.axis_size(axis), *array.shape))
-    return lax.all_to_all(copies, axis, split_axis=0, concat_axis=0, tiled=True)
-
-
-def collect(array, axis, dim):
-    return in_order(copy_for_each(array, axis), dim)
-
-
-def side_by_side(arrays, axis, dim, along):
-    both = jnp.concatenate(arrays, axis=along)
-    out, at, done = (lax.all_gather(both, axis, axis=dim, tiled=True), 0, [])
-    for a in arrays:
-        done.append(lax.slice_in_dim(out, at, at + a.shape[along], axis=along))
-        at += a.shape[along]
-    return tuple(done)
-
-
-def summed_on_arrival(array, axis, dim):
-    blocks = cut_along(array, dim, lax.axis_size(axis))
-    arrived = lax.all_to_all(blocks, axis, split_axis=0, concat_axis=0, tiled=True)
-    return arrived.astype(jnp.float32).sum(axis=0)
+def shifted(array, axis, by):
+    count = lax.axis_size(axis)
+    return lax.ppermute(array, axis, [(i, (i + by) % count) for i in range(count)])
+
+
+def added(*terms):
+    return sum((t.astype(jnp.float32) for t in terms[1:]), terms[0].astype(jnp.float32))
+
+
+def settle_kernel(own_ref, top_ref, top2_ref, low_ref, low2_ref, out_ref):
+    half = top_ref.shape[0]
+    out_ref[:half] = added(own_ref[:half], top_ref[...], top2_ref[...]).astype(out_ref.dtype)
+    out_ref[half:] = added(own_ref[half:], low_ref[...], low2_ref[...]).astype(out_ref.dtype)
+
+
+def settle(own, tops, lows):
+    vmem = pl.BlockSpec(memory_space=pltpu.VMEM)
+    return pl.pallas_call(
+        settle_kernel,
+        in_specs=[vmem] * 5,
+        out_specs=vmem,
+        out_shape=jax.ShapeDtypeStruct(own.shape, jnp.bfloat16),
+        cost_estimate=pl.CostEstimate(
+            flops=2 * own.size, bytes_accessed=10 * own.size, transcendentals=0
+        ),
+        compiler_params=pltpu.CompilerParams(vmem_limit_bytes=12 << 20),
+        name="settle",
+    )(own, *tops, *lows)
+
+
+def relayed(far_in, mine):
+    return added(mine, far_in).astype(jnp.bfloat16)
+
+
+def ring_places(axis):
+    count = lax.axis_size(axis)
+    me = lax.axis_index(axis)
+    return jnp.stack([(me + by) % count for by in (2, 1, count - 1, 0)]).astype(jnp.int32)
+
+
+def ring_sum(far, right, left, own, axis):
+    far_top_in = shifted(far[0], axis, 1)
+    far_low_in = shifted(far[1], axis, -1)
+    right_low_in = shifted(right[1], axis, 1)
+    left_top_in = shifted(left[0], axis, -1)
+    relay_top_in = shifted(relayed(far_top_in, right[0]), axis, 1)
+    relay_low_in = shifted(relayed(far_low_in, left[1]), axis, -1)
+    return settle(own, (left_top_in, relay_top_in), (right_low_in, relay_low_in))
+
+
+def project_kernel(places_ref, rows_ref, weight_ref, base_ref, *outs):
+    half = outs[0].shape[0]
+    step = pl.program_id(0)
+    terms = jnp.dot(rows_ref[...], weight_ref[...], preferred_element_type=jnp.float32)
+    for k in range(3):
+
+        @pl.when(step == k)
+        def _(k=k):
+            outs[2 * k][...] = terms[:half].astype(jnp.bfloat16)
+            outs[2 * k + 1][...] = terms[half:].astype(jnp.bfloat16)
+
+    @pl.when(step == 3)
+    def _():
+        outs[6][...] = terms + base_ref[...].astype(jnp.float32)
+
+
+def project(places, rows, weight, base):
+    tok, inner = rows.shape
+    width = base.shape[1]
+    piece = pl.BlockSpec((tok // 2, width), lambda j, o: (0, 0))
+    whole = pl.BlockSpec((tok, width), lambda j, o: (0, 0))
+    outs = pl.pallas_call(
+        project_kernel,
+        grid_spec=pltpu.PrefetchScalarGridSpec(
+            num_scalar_prefetch=1,
+            grid=(4,),
+            in_specs=[
+                pl.BlockSpec((tok, inner), lambda j, o: (0, 0)),
+                pl.BlockSpec((inner, width), lambda j, o: (0, o[j])),
+                whole,
+            ],
+            out_specs=[piece] * 6 + [whole],
+        ),
+        out_shape=[jax.ShapeDtypeStruct((tok // 2, width), jnp.bfloat16)] * 6
+        + [jax.ShapeDtypeStruct((tok, width), jnp.float32)],
+        cost_estimate=pl.CostEstimate(
+            flops=8 * tok * inner * width,
+            bytes_accessed=2 * tok * inner + 8 * inner * width + 12 * tok * width,
+            transcendentals=0,
+        ),
+        compiler_params=pltpu.CompilerParams(vmem_limit_bytes=24 << 20),
+        name="project",
+    )(places, rows, weight, base)
+    return (outs[0:2], outs[2:4], outs[4:6], outs[6])
+
+
+def norm_kernel(places_ref, gain_ref, own_ref, left_ref, right_ref, top_ref, low_ref, out_ref):
+    width = own_ref.shape[1]
+    half = top_ref.shape[0]
+    model = out_ref.shape[1]
+    for at, far_ref in ((0, top_ref), (half, low_ref)):
+        parts = [
+            ref[pl.ds(at, half), :].astype(jnp.float32) for ref in (own_ref, left_ref, right_ref)
+        ]
+        parts = [far_ref[...].astype(jnp.float32), parts[2], parts[1], parts[0]]
+        square = sum(jnp.sum(p * p, axis=-1, keepdims=True) for p in parts)
+        scale = lax.rsqrt(square / model + 1e-06)
+        for k, part in enumerate(parts):
+            place = places_ref[k]
+            gain = gain_ref[pl.ds(place, 1), :]
+            columns = pl.ds(pl.multiple_of(place * width, width), width)
+            out_ref[pl.ds(at, half), columns] = (part * scale * gain).astype(out_ref.dtype)
+
+
+def normalised(places, gain, own, axis):
+    tok, width = own.shape
+    half = tok // 2
+    left, right = (shifted(own, axis, 1), shifted(own, axis, -1))
+    far_top = shifted(left[:half], axis, 1)
+    far_low = shifted(right[half:], axis, -1)
+    vmem = pl.BlockSpec(memory_space=pltpu.VMEM)
+    model = gain.shape[0]
+    return pl.pallas_call(
+        norm_kernel,
+        in_specs=[pl.BlockSpec(memory_space=pltpu.SMEM)] + [vmem] * 6,
+        out_specs=vmem,
+        out_shape=jax.ShapeDtypeStruct((tok, model), jnp.bfloat16),
+        cost_estimate=pl.CostEstimate(
+            flops=6 * tok * model, bytes_accessed=4 * tok * model, transcendentals=tok
+        ),
+        compiler_params=pltpu.CompilerParams(vmem_limit_bytes=24 << 20),
+        name="norm",
+    )(places, gain.reshape(model // width, width), own, left, right, far_top, far_low)
+
+
+def times_transposed(rows, columns):
+    return lax.dot_general(
+        rows, columns, (((1,), (1,)), ((), ())), preferred_element_type=jnp.float32
+    )
+
+
+def held(array):
+    return pltpu.with_memory_space_constraint(array, pltpu.VMEM)
+
+
+def hold(shape, dtype=jnp.bfloat16):
+    return pltpu.VMEM(shape, dtype)
+
+
+CHUNK = 256
+
+
+def hide(normed_ref, both_ref, hidden_ref, low, at, size):
+    rows = hidden_ref.shape[0]
+    product = jnp.dot(
+        normed_ref[low : low + rows, :],
+        both_ref[:, pl.ds(2 * at, 2 * size)],
+        preferred_element_type=jnp.float32,
+    )
+    gate = product[:, :size]
+    up = product[:, size:]
+    hidden_ref[:, pl.ds(at, size)] = (gate / (1.0 + jnp.exp(-gate)) * up).astype(jnp.bfloat16)
+
+
+def two_shares(hidden_ref, down_ref, which, outs):
+    def body(i, carry):
+        terms = times_transposed(hidden_ref[...], down_ref[jnp.where(i == 0, *which)])
+        for j in range(2):
+
+            @pl.when(i == j)
+            def _(j=j):
+                outs[j][...] = terms.astype(jnp.bfloat16)
+
+        return carry
+
+    lax.fori_loop(0, 2, body, 0)
+
+
+def top_kernel(places_ref, normed_ref, weights_ref, *rest):
+    hidden_ref, far_ref, left_ref, both_ref, down_ref, sems, down_sems = rest
+    units = hidden_ref.shape[1]
+    owned = far_ref.shape[1]
+    count, first = divmod(units, CHUNK)
+
+    def copies(slot, at, size):
+        return [
+            pltpu.make_async_copy(
+                weights_ref.at[:, pl.ds(k * units + at, size)],
+                both_ref.at[:, pl.ds(2 * at + k * size, size)],
+                sems.at[slot, k],
+            )
+            for k in range(2)
+        ]
+
+    def down_copy(k):
+        row = pl.multiple_of(places_ref[k] * owned, owned)
+        return pltpu.make_async_copy(
+            weights_ref.at[pl.ds(row, owned), pl.ds(2 * units, units)],
+            down_ref.at[k],
+            down_sems.at[k],
+        )
+
+    for copy in copies(0, 0, first):
+        copy.start()
+    for i in range(count):
+        for copy in copies(1 + i, first + i * CHUNK, CHUNK):
+            copy.start()
+    for k in range(4):
+        down_copy(k).start()
+    for copy in copies(0, 0, first):
+        copy.wait()
+    hide(normed_ref, both_ref, hidden_ref, 0, 0, first)
+
+    def body(i, carry):
+        at = pl.multiple_of(first + i * CHUNK, 128)
+        for copy in copies(1 + i, at, CHUNK):
+            copy.wait()
+        hide(normed_ref, both_ref, hidden_ref, 0, at, CHUNK)
+        return carry
+
+    lax.fori_loop(0, count, body, 0)
+    for k in range(4):
+        down_copy(k).wait()
+    two_shares(hidden_ref, down_ref, (0, 2), (far_ref, left_ref))
+
+
+def low_kernel(normed_ref, both_ref, down_ref, hidden_ref, far_ref, right_ref):
+    count, first = divmod(hidden_ref.shape[1], CHUNK)
+    rows = hidden_ref.shape[0]
+    hide(normed_ref, both_ref, hidden_ref, rows, 0, first)
+
+    def body(i, carry):
+        at = pl.multiple_of(first + i * CHUNK, 128)
+        hide(normed_ref, both_ref, hidden_ref, rows, at, CHUNK)
+        return carry
+
+    lax.fori_loop(0, count, body, 0)
+    two_shares(hidden_ref, down_ref, (0, 1), (far_ref, right_ref))
+
+
+def rest_kernel(top_ref, low_ref, down_ref, right_ref, left_ref):
+    right_ref[...] = times_transposed(top_ref[...], down_ref[1]).astype(jnp.bfloat16)
+    left_ref[...] = times_transposed(low_ref[...], down_ref[2]).astype(jnp.bfloat16)
+
+
+def own_kernel(top_ref, low_ref, down_ref, base_ref, out_ref):
+    half = top_ref.shape[0]
+    for at, hidden_ref in ((0, top_ref), (half, low_ref)):
+        terms = times_transposed(hidden_ref[...], down_ref[3])
+        out_ref[at : at + half] = terms + base_ref[at : at + half].astype(jnp.float32)
+
+
+def feed_forward(places, normed, weights, base, axis):
+    tok, model = normed.shape
+    owned = base.shape[1]
+    units = weights.shape[1] // 3
+    half = tok // 2
+    vmem = pl.BlockSpec(memory_space=pltpu.VMEM)
+    part, hid = ((half, owned), (half, units))
+    cost = pl.CostEstimate(
+        flops=2 * tok * model * units, bytes_accessed=6 * model * units, transcendentals=half * units
+    )
+    small = pl.CostEstimate(
+        flops=2 * tok * units * owned, bytes_accessed=4 * tok * owned, transcendentals=0
+    )
+    grant = pltpu.CompilerParams(vmem_limit_bytes=20 << 20)
+    normed = held(normed)
+    top, far_top, left_top, both, down = pl.pallas_call(
+        top_kernel,
+        in_specs=[
+            pl.BlockSpec(memory_space=pltpu.SMEM),
+            vmem,
+            pl.BlockSpec(memory_space=pltpu.HBM),
+        ],
+        out_specs=[vmem] * 5,
+        out_shape=[
+            hold(hid),
+            hold(part),
+            hold(part),
+            hold((model, 2 * units)),
+            hold((4, owned, units)),
+        ],
+        scratch_shapes=[
+            pltpu.SemaphoreType.DMA((1 + units // CHUNK, 2)),
+            pltpu.SemaphoreType.DMA((4,)),
+        ],
+        cost_estimate=cost,
+        compiler_params=grant,
+        name="top",
+    )(places, normed, weights)
+    down = held(down)
+    far_top_in = shifted(far_top, axis, 1)
+    left_top_in = shifted(left_top, axis, -1)
+    low_half = pl.pallas_call(
+        low_kernel,
+        in_specs=[vmem] * 3,
+        out_specs=[vmem] * 3,
+        out_shape=[hold(hid), hold(part), hold(part)],
+        cost_estimate=cost,
+        compiler_params=grant,
+        name="low",
+    )
+    both = held(both)
+    low, far_low, right_low = low_half(normed, both, down)
+    far_low_in = shifted(far_low, axis, -1)
+    right_low_in = shifted(right_low, axis, 1)
+    top, low = (held(top), held(low))
+    rest = pl.pallas_call(
+        rest_kernel,
+        in_specs=[vmem] * 3,
+        out_specs=[vmem] * 2,
+        out_shape=[hold(part)] * 2,
+        cost_estimate=small,
+        compiler_params=grant,
+        name="rest",
+    )
+    right_top, left_low = rest(top, low, down)
+    relay_top = relayed(far_top_in, right_top)
+    relay_top_in = shifted(relay_top, axis, 1)
+    relay_low = relayed(far_low_in, left_low)
+    relay_low_in = shifted(relay_low, axis, -1)
+    own = pl.pallas_call(
+        own_kernel,
+        in_specs=[vmem] * 4,
+        out_specs=vmem,
+        out_shape=hold((tok, owned), jnp.float32),
+        cost_estimate=small,
+        compiler_params=grant,
+        name="own",
+    )(top, low, down, base)
+    return pl.pallas_call(
+        settle_kernel,
+        in_specs=[vmem] * 5,
+        out_specs=vmem,
+        out_shape=jax.ShapeDtypeStruct((tok, owned), jnp.bfloat16),
+        cost_estimate=pl.CostEstimate(
+            flops=2 * tok * owned, bytes_accessed=10 * tok * owned, transcendentals=0
+        ),
+        compiler_params=pltpu.CompilerParams(vmem_limit_bytes=12 << 20),
+        name="close",
+    )(held(own), left_top_in, relay_top_in, right_low_in, relay_low_in)
 
 
 def rotate(values, positions):
@@ -89,6 +394,8 @@
 def body(
     resid, queries, keys_values, sink, out_weight, norm_gain, gate_weight, up_weight, down_weight
 ):
+    shard = jnp.concatenate((gate_weight, up_weight, down_weight.T), axis=1)
+    weights = lax.all_gather(shard, "sp", axis=0, tiled=True)
     tok = queries.shape[0]
     heads_here = queries.shape[1] // HEAD_DIM
     kv_here = keys_values.shape[1]
@@ -130,23 +437,11 @@
         "nkgqj,njkd->nqkgd", probs, key_blocks[..., HEAD_DIM:], preferred_element_type=jnp.float32
     )
     attended = attended.astype(jnp.bfloat16).reshape(tok, heads_here * HEAD_DIM)
-    partial_proj = jnp.dot(attended, out_weight, preferred_element_type=jnp.float32)
-    projected = summed_on_arrival(partial_proj.astype(jnp.bfloat16), "tp", 1)
-    stream_cols = (resid.astype(jnp.float32) + projected).astype(jnp.bfloat16)
-    stream = collect(stream_cols, "tp", 1)
-    widened = stream.astype(jnp.float32)
-    normed = (
-        widened * lax.rsqrt(jnp.mean(widened * widened, axis=-1, keepdims=True) + 1e-06) * norm_gain
-    ).astype(jnp.bfloat16)
-    pieces = side_by_side((gate_weight, up_weight, down_weight.T), "sp", 0, 1)
-    gate = jnp.dot(normed, pieces[0], preferred_element_type=jnp.float32)
-    up = jnp.dot(normed, pieces[1], preferred_element_type=jnp.float32)
-    hidden = lax.optimization_barrier((jax.nn.silu(gate) * up).astype(jnp.bfloat16))
-    terms = lax.dot_general(
-        hidden, pieces[2], (((1,), (1,)), ((), ())), preferred_element_type=jnp.float32
-    )
-    summed = summed_on_arrival(terms.astype(jnp.bfloat16), "tp", 1)
-    return (stream_cols.astype(jnp.float32) + summed).astype(jnp.bfloat16)
+    places = ring_places("tp")
+    far, right, left, own = project(places, attended, out_weight, resid)
+    stream = ring_sum(far, right, left, own, "tp")
+    normed = normalised(places, norm_gain, stream, "tp")
+    return feed_forward(places, normed, weights, stream, "tp")
 
 
 def solution(mesh):

time: 195 us -> 184 us (0.944)
  blocking collectives: 104 us -> 0 us
  waiting for transfers between devices: 5.63 us -> 70 us
  Pallas kernels: 0 us -> 23.3 us
  starting transfers between devices: 23.6 us -> 46.3 us
  matrix products: 23.8 us -> 4.33 us
  local copies, waits for them, and re-layouts: 11.6 us -> 18.8 us
  other arithmetic: 12 us -> 6.69 us
    all_to_all x3 -> x0, blocking collectives: 104 us -> none  [the longest x2 70.3 us: summed_on_arrival(): lax.all_to_all(blocks, axis, split_axis=0, concat_axis=0, tiled=True)]
    ppermute x0 -> x16, waiting for transfers between devices: none -> 54.4 us  [shifted(): lax.ppermute(array, axis, [(i, (i + by) % count) for i in range(count)])]
    pallas_call x0 -> x8, Pallas kernels: none -> 23.3 us  [the longest x1 8.47 us: feed_forward(): pl.pallas_call(top_kernel, in_specs=[pl.BlockSpec(memory_space=pltpu.SMEM...]
    ppermute x0 -> x16, starting transfers between devices: none -> 21.9 us  [shifted(): lax.ppermute(array, axis, [(i, (i + by) % count) for i in range(count)])]
    dot_general x4 -> x0, matrix products: 19.2 us -> none  [the longest x1 8.05 us: body(): gate = jnp.dot(normed, pieces[0], preferred_element_type=jnp.float32)]
    all_gather x1, waiting for transfers between devices: 5.57 us -> 15.6 us  [body(): weights = lax.all_gather(shard, 'sp', axis=0, tiled=True)]
    unnamed x20 -> x28, local copies, waits for them, and re-layouts: 3.18 us -> 9.45 us
    reshape x2 -> x3, local copies, waits for them, and re-layouts: 0.48 us -> 5.9 us  [the longest x2 5.89 us: body(): attended = attended.astype(jnp.bfloat16).reshape(tok, heads_here * HEAD_DIM)]
  transfers between devices with their start and end apart: 3 -> 19, of which waited for: 1 -> 12; matrix products, arithmetic and copies ran while one was open for 13% -> 11% of each run, Pallas kernels for 0% -> 4%
where the time goes in v2:
time: 184 us; the launch traced here: 183 us
  waiting for transfers between devices  70 us (38%)
  starting transfers between devices  46.3 us (25%)
  Pallas kernels  23.3 us (13%)
  local copies, waits for them, and re-layouts  18.8 us (10%)
  between operations  13.9 us (8%)
  other arithmetic  6.69 us (4%)
  matrix products  4.33 us (2%)
    ppermute x16, waiting for transfers between devices, shifted(): lax.ppermute(array, axis, [(i, (i + by) % count) for i in range(count)])  54.4 us
    ppermute x1, starting transfers between devices, with_halo(): lax.ppermute(head, axis, [((i + 1) % count, i) for i in range(ends)])  22.4 us
    ppermute x16, starting transfers between devices, shifted(): lax.ppermute(array, axis, [(i, (i + by) % count) for i in range(count)])  21.9 us
    all_gather x1, waiting for transfers between devices, body(): weights = lax.all_gather(shard, 'sp', axis=0, tiled=True)  15.6 us
    unnamed x28, local copies, waits for them, and re-layouts  9.45 us
    pallas_call x1, Pallas kernels, feed_forward(): pl.pallas_call(top_kernel, in_specs=[pl.BlockSpec(memory_space=pltpu.SMEM...  8.47 us
    pallas_call x1, Pallas kernels, feed_forward(): low, far_low, right_low = low_half(normed, both, down)  6.39 us
    reshape x2, local copies, waits for them, and re-layouts, body(): attended = attended.astype(jnp.bfloat16).reshape(tok, heads_here * HEAD_DIM)  5.89 us
  transfers between devices with their start and end apart: 19, of which 12 were waited for; matrix products, arithmetic and copies ran while one was open for 11% of the time, Pallas kernels for 4%

profile of v2, /device:TPU:33, one launch (start us, length us, event | category | flops | bytes accessed | tf_op | source)
XLA Modules:
  0.0 183.2 jit_solution(2429563762480404396)
XLA Ops:
  11.2 22.4 %collective-permute-start.1 = (bf16[128,2,128]{0,2,1:T(8,128)(2,1)S(1)}, bf16[128,2,128]{0,2,1:T(8,128)(2,1)S(1)}, u32[]{:S(2)}, u32[]{:S(2)}) collective-permute-start(bf16[128,2,128]{0,2,1:T(8,128)(2,1)S(1)} %get-tuple-element.45), channel_id=1, source_target_pairs={{4,0},{8,4},{12,8},{16,12},{20,16},{24,20},{28,24},{32,28},{36,32}... | collective-permute-start | bytes 196616 | tf_op jit(solution)/shard_map/ppermute | solution.py:24
  44.1 3.1 %fusion.4 = bf16[5,128,2,4,64]{1,4,3,2,0:T(8,128)(2,1)} fusion(f32[5,2,384,128,4]{3,2,4,1,0:T(8,128)S(1)} %get-tuple-element.58, f32[5,2,4,128]{3,2,1,0:T(4,128)S(1)} %exponential_add_fusion, f32[5,2,4,128]{3,2,1,0:T(4,128)S(1)} %broadcast_maximum_fusion, pred[5,128,384]{1,2,0:T(8,128)(4,1)S(1)} %fusion.6, bf16[5,384,2,128]{1,3,2,0:T(8,128)(2,1)S(1)} %fusion.16), kind=kOutput, calls=%fused_computation.7 | convolution fusion | flops 261816320 | bytes 9297920 | tf_op jit(solution)/shard_map/nkgqj,njkd->nqkgd/dot_general | solution.py:436
  47.1 3.3 %copy.31 = bf16[5,128,2,4,64]{4,3,2,1,0:T(4,128)(2,1)} copy(bf16[5,128,2,4,64]{1,4,3,2,0:T(8,128)(2,1)} %fusion.4) | data formatting | bytes 1310720 | tf_op jit(solution)/shard_map/reshape | solution.py:439
  50.4 2.6 %reshape.259.rows_ref = bf16[640,512]{1,0:T(8,128)(2,1)S(1)} reshape(bf16[5,128,2,4,64]{4,3,2,1,0:T(4,128)(2,1)} %copy.31) | data formatting | bytes 1310720 | tf_op jit(solution)/shard_map/reshape | solution.py:439
  54.2 3.1 %project.1 = (bf16[320,512]{1,0:T(8,128)(2,1)S(1)}, bf16[320,512]{1,0:T(8,128)(2,1)S(1)}, bf16[320,512]{1,0:T(8,128)(2,1)S(1)}, bf16[320,512]{1,0:T(8,128)(2,1)S...) custom-call(s32[4]{0:T(128)S(1)} %pad_add_fusion.places_ref, ...), custom_call_target="tpu_custom_call" | custom-call | flops 1342177280 | bytes 6684672 | tf_op jit(solution)/shard_map/project/pallas_call | solution.py:102
  57.4 2.7 %collective-permute-start.6 = (bf16[320,512]{1,0:T(8,128)(2,1)S(1)}, bf16[320,512]{1,0:T(8,128)(2,1)S(1)}, u32[]{:S(2)}, u32[]{:S(2)}) collective-permute-start(bf16[320,512]{1,0:T(8,128)(2,1)S(1)} %get-tuple-element.28), channel_id=1, source_target_pairs={{0,3},{1,0},{2,1},{3,2},{4,7},{5,4},{6,5},{7,6},{8,11},{9,8},{10,9... | collective-permute-start | bytes 983048 | tf_op jit(solution)/shard_map/ppermute | solution.py:33
  61.6 6.0 %collective-permute-done.3 = bf16[320,512]{1,0:T(8,128)(2,1)S(1)} collective-permute-done((bf16[320,512]{1,0:T(8,128)(2,1)S(1)}, bf16[320,512]{1,0:T(8,128)(2,1)S(1)}, u32[]{:S(2)}, u32[]{:S(2)}) %collective-permute-start.3) | collective-permute-done | bytes 327712 | tf_op jit(solution)/shard_map/ppermute | solution.py:33
  67.9 2.8 %collective-permute-start.7 = (bf16[320,512]{1,0:T(8,128)(2,1)S(1)}, bf16[320,512]{1,0:T(8,128)(2,1)S(1)}, u32[]{:S(2)}, u32[]{:S(2)}) collective-permute-start(bf16[320,512]{1,0:T(8,128)(2,1)S(1)} %add_convert_fusion.2), channel_id=1, source_target_pairs={{0,3},{1,0},{2,1},{3,2},{4,7},{5,4},{6,5},{7,6},{8,11},{9,8},{10,9... | collective-permute-start | bytes 983048 | tf_op jit(solution)/shard_map/ppermute | solution.py:33
  70.7 3.0 %collective-permute-done.2.top_ref = bf16[320,512]{1,0:T(8,128)(2,1)S(1)} collective-permute-done((bf16[320,512]{1,0:T(8,128)(2,1)S(1)}, bf16[320,512]{1,0:T(8,128)(2,1)S(1)}, u32[]{:S(2)}, u32[]{:S(2)}) %collective-permute-start.2) | collective-permute-done | bytes 327712 | tf_op jit(solution)/shard_map/ppermute | solution.py:33
  74.6 7.0 %collective-permute-done.4.top2_ref = bf16[320,512]{1,0:T(8,128)(2,1)S(1)} collective-permute-done((bf16[320,512]{1,0:T(8,128)(2,1)S(1)}, bf16[320,512]{1,0:T(8,128)(2,1)S(1)}, u32[]{:S(2)}, u32[]{:S(2)}) %collective-permute-start.4) | collective-permute-done | bytes 327712 | tf_op jit(solution)/shard_map/ppermute | solution.py:33
  81.8 2.5 %collective-permute-start.9 = (bf16[640,512]{1,0:T(8,128)(2,1)S(1)}, bf16[640,512]{1,0:T(8,128)(2,1)S(1)}, u32[]{:S(2)}, u32[]{:S(2)}) collective-permute-start(bf16[640,512]{1,0:T(8,128)(2,1)S(1)} %settle.1.own_ref.base_ref), channel_id=1, source_target_pairs={{0,3},{1,0},{2,1},{3,2},{4,7},{5,4},{6,5},{7,6},{8,11},{9,8},{10,9... | collective-permute-start | bytes 1966088 | tf_op jit(solution)/shard_map/ppermute | solution.py:33
  84.3 12.8 %collective-permute-done.9.right_ref = bf16[640,512]{1,0:T(8,128)(2,1)S(1)} collective-permute-done((bf16[640,512]{1,0:T(8,128)(2,1)S(1)}, bf16[640,512]{1,0:T(8,128)(2,1)S(1)}, u32[]{:S(2)}, u32[]{:S(2)}) %collective-permute-start.9) | collective-permute-done | bytes 655392 | tf_op jit(solution)/shard_map/ppermute | solution.py:33
  97.2 3.4 %collective-permute-start.11 = (bf16[320,512]{1,0:T(8,128)(2,1)S(1)}, bf16[320,512]{1,0:T(8,128)(2,1)S(1)}, u32[]{:S(2)}, u32[]{:S(2)}) collective-permute-start(bf16[320,512]{1,0:T(8,128)(2,1)S(1)} %slice.114), channel_id=1, source_target_pairs={{0,3},{1,0},{2,1},{3,2},{4,7},{5,4},{6,5},{7,6},{8,11},{9,8},{10,9... | collective-permute-start | bytes 983048 | tf_op jit(solution)/shard_map/ppermute | solution.py:33
  101.5 4.0 %collective-permute-done.11.low_ref = bf16[320,512]{1,0:T(8,128)(2,1)S(1)} collective-permute-done((bf16[320,512]{1,0:T(8,128)(2,1)S(1)}, bf16[320,512]{1,0:T(8,128)(2,1)S(1)}, u32[]{:S(2)}, u32[]{:S(2)}) %collective-permute-start.11) | collective-permute-done | bytes 327712 | tf_op jit(solution)/shard_map/ppermute | solution.py:33
  106.2 3.3 %collective-permute-done.10.top_ref = bf16[320,512]{1,0:T(8,128)(2,1)S(1)} collective-permute-done((bf16[320,512]{1,0:T(8,128)(2,1)S(1)}, bf16[320,512]{1,0:T(8,128)(2,1)S(1)}, u32[]{:S(2)}, u32[]{:S(2)}) %collective-permute-start.10) | collective-permute-done | bytes 327712 | tf_op jit(solution)/shard_map/ppermute | solution.py:33
  116.1 15.6 %all-gather.2.cloned.1.call-done.weights_ref = bf16[2048,4224]{1,0:T(8,128)(2,1)} async-done(((bf16[64,4224]{1,0:T(8,128)(2,1)}), bf16[2048,4224]{1,0:T(8,128)(2,1)}) %all-gather.2.cloned.1.call-update) | async-done | bytes 17301520 | tf_op jit(solution)/shard_map/all_gather | solution.py:398
  131.7 8.5 %top.1 = (bf16[320,1408]{1,0:T(8,128)(2,1)S(1)}, bf16[320,512]{1,0:T(8,128)(2,1)S(1)}, bf16[320,512]{1,0:T(8,128)(2,1)S(1)}, bf16[2048,2816]{1,0:T(8,128)(2,1)S(1)}, bf16[4,512,1408]{2,1,0:T(8,128)(2,1)S(1)}) custom-call(s32[4]{0:T(128)S(1)} %pad_add_fusion.places_ref, bf16[640,2048]{1,0:T(8,128)(2,1)S(1)} %norm.1.normed_ref, ...), custom_call_target="tpu_custom_call" | custom-call | flops 3690987520 | bytes 17301504 | tf_op jit(solution)/shard_map/top/pallas_call | solution.py:298
  140.2 6.4 %low.1 = (bf16[320,1408]{1,0:T(8,128)(2,1)S(1)}, bf16[320,512]{1,0:T(8,128)(2,1)S(1)}, bf16[320,512]{1,0:T(8,128)(2,1)S(1)}) custom-call(bf16[640,2048]{1,0:T(8,128)(2,1)S(1)} %norm.1.normed_ref, bf16[2048,2816]{1,0:T(8,128)(2,1)S(1)} %get-tuple-element.30.both_ref, bf16[4,512,1408]{2,1,0:T(8,128)(2,1)S(1)} %get-tuple-element.31.down_ref), custom_call_target="tpu_custom_call" | custom-call | flops 3690987520 | bytes 17301504 | tf_op jit(solution)/shard_map/low/pallas_call | solution.py:334
  146.6 2.5 %collective-permute-start.16 = (bf16[320,512]{1,0:T(8,128)(2,1)S(1)}, bf16[320,512]{1,0:T(8,128)(2,1)S(1)}, u32[]{:S(2)}, u32[]{:S(2)}) collective-permute-start(bf16[320,512]{1,0:T(8,128)(2,1)S(1)} %get-tuple-element.38), channel_id=1, source_target_pairs={{0,3},{1,0},{2,1},{3,2},{4,7},{5,4},{6,5},{7,6},{8,11},{9,8},{10,9... | collective-permute-start | bytes 983048 | tf_op jit(solution)/shard_map/ppermute | solution.py:33
  149.1 2.7 %collective-permute-start.12 = (bf16[320,512]{1,0:T(8,128)(2,1)S(1)}, bf16[320,512]{1,0:T(8,128)(2,1)S(1)}, u32[]{:S(2)}, u32[]{:S(2)}) collective-permute-start(bf16[320,512]{1,0:T(8,128)(2,1)S(1)} %get-tuple-element.33), channel_id=1, source_target_pairs={{0,3},{1,0},{2,1},{3,2},{4,7},{5,4},{6,5},{7,6},{8,11},{9,8},{10,9... | collective-permute-start | bytes 983048 | tf_op jit(solution)/shard_map/ppermute | solution.py:33
  153.0 2.9 %collective-permute-done.16 = bf16[320,512]{1,0:T(8,128)(2,1)S(1)} collective-permute-done((bf16[320,512]{1,0:T(8,128)(2,1)S(1)}, bf16[320,512]{1,0:T(8,128)(2,1)S(1)}, u32[]{:S(2)}, u32[]{:S(2)}) %collective-permute-start.16) | collective-permute-done | bytes 327712 | tf_op jit(solution)/shard_map/ppermute | solution.py:33
  156.0 3.5 %collective-permute-start.17 = (bf16[320,512]{1,0:T(8,128)(2,1)S(1)}, bf16[320,512]{1,0:T(8,128)(2,1)S(1)}, u32[]{:S(2)}, u32[]{:S(2)}) collective-permute-start(bf16[320,512]{1,0:T(8,128)(2,1)S(1)} %add_convert_fusion), channel_id=1, source_target_pairs={{0,3},{1,0},{2,1},{3,2},{4,7},{5,4},{6,5},{7,6},{8,11},{9,8},{10,9... | collective-permute-start | bytes 983048 | tf_op jit(solution)/shard_map/ppermute | solution.py:33
  159.5 6.5 %collective-permute-done.13 = bf16[320,512]{1,0:T(8,128)(2,1)S(1)} collective-permute-done((bf16[320,512]{1,0:T(8,128)(2,1)S(1)}, bf16[320,512]{1,0:T(8,128)(2,1)S(1)}, u32[]{:S(2)}, u32[]{:S(2)}) %collective-permute-start.13) | collective-permute-done | bytes 327712 | tf_op jit(solution)/shard_map/ppermute | solution.py:33
  170.0 5.4 %collective-permute-done.14.top2_ref = bf16[320,512]{1,0:T(8,128)(2,1)S(1)} collective-permute-done((bf16[320,512]{1,0:T(8,128)(2,1)S(1)}, bf16[320,512]{1,0:T(8,128)(2,1)S(1)}, u32[]{:S(2)}, u32[]{:S(2)}) %collective-permute-start.14) | collective-permute-done | bytes 327712 | tf_op jit(solution)/shard_map/ppermute | solution.py:33
  (96 shorter events, 33.4 us)
Async XLA Ops:
  6.5 125.2 %all-gather.2.cloned.1.call-start = ((), (), s32[]{:S(2)}) async-start(), calls=%async_computation | async-start | bytes 17842176 | tf_op jit(solution)/shard_map/all_gather | solution.py:398
  11.2 29.4 %collective-permute-start.1 = (bf16[128,2,128]{0,2,1:T(8,128)(2,1)S(1)}, bf16[128,2,128]{0,2,1:T(8,128)(2,1)S(1)}, u32[]{:S(2)}, u32[]{:S(2)}) collective-permute-start(bf16[128,2,128]{0,2,1:T(8,128)(2,1)S(1)} %get-tuple-element.45), channel_id=1, source_target_pairs={{4,0},{8,4},{12,8},{16,12},{20,16},{24,20},{28,24},{32,28},{36,32}... | collective-permute-start | bytes 196616 | tf_op jit(solution)/shard_map/ppermute | solution.py:24
  33.6 6.9 %collective-permute-start = (bf16[128,2,128]{0,2,1:T(8,128)(2,1)S(1)}, bf16[128,2,128]{0,2,1:T(8,128)(2,1)S(1)}, u32[]{:S(2)}, u32[]{:S(2)}) collective-permute-start(bf16[128,2,128]{0,2,1:T(8,128)(2,1)S(1)} %get-tuple-element.46), channel_id=1, source_target_pairs={{0,4},{4,8},{8,12},{12,16},{16,20},{20,24},{24,28},{28,32},{32,36}... | collective-permute-start | bytes 196616 | tf_op jit(solution)/shard_map/ppermute | solution.py:22
  44.0 9.0 %copy-start.8 = (bf16[512,2048]{1,0:T(8,128)(2,1)S(1)}, bf16[512,2048]{1,0:T(8,128)(2,1)}, u32[]{:S(2)}) copy-start(bf16[512,2048]{1,0:T(8,128)(2,1)} %weight_ref.1) | copy-start | bytes 6291460
  47.1 54.3 %copy-start.10 = (f32[2048]{0:T(1024)S(1)}, f32[2048]{0:T(1024)}, u32[]{:S(2)}) copy-start(f32[2048]{0:T(1024)} %param.14) | copy-start | bytes 24580
  53.0 1.1 copy-start.9
  57.3 10.3 %collective-permute-start.3 = (bf16[320,512]{1,0:T(8,128)(2,1)S(1)}, bf16[320,512]{1,0:T(8,128)(2,1)S(1)}, u32[]{:S(2)}, u32[]{:S(2)}) collective-permute-start(bf16[320,512]{1,0:T(8,128)(2,1)S(1)} %get-tuple-element.25), channel_id=1, source_target_pairs={{0,1},{1,2},{2,3},{3,0},{4,5},{5,6},{6,7},{7,4},{8,9},{9,10},{10,1... | collective-permute-start | bytes 983048 | tf_op jit(solution)/shard_map/ppermute | solution.py:33
  57.4 10.4 %collective-permute-start.6 = (bf16[320,512]{1,0:T(8,128)(2,1)S(1)}, bf16[320,512]{1,0:T(8,128)(2,1)S(1)}, u32[]{:S(2)}, u32[]{:S(2)}) collective-permute-start(bf16[320,512]{1,0:T(8,128)(2,1)S(1)} %get-tuple-element.28), channel_id=1, source_target_pairs={{0,3},{1,0},{2,1},{3,2},{4,7},{5,4},{6,5},{7,6},{8,11},{9,8},{10,9... | collective-permute-start | bytes 983048 | tf_op jit(solution)/shard_map/ppermute | solution.py:33
  60.1 13.6 %collective-permute-start.2 = (bf16[320,512]{1,0:T(8,128)(2,1)S(1)}, bf16[320,512]{1,0:T(8,128)(2,1)S(1)}, u32[]{:S(2)}, u32[]{:S(2)}) collective-permute-start(bf16[320,512]{1,0:T(8,128)(2,1)S(1)} %get-tuple-element.23), channel_id=1, source_target_pairs={{0,3},{1,0},{2,1},{3,2},{4,7},{5,4},{6,5},{7,6},{8,11},{9,8},{10,9... | collective-permute-start | bytes 983048 | tf_op jit(solution)/shard_map/ppermute | solution.py:33
  60.1 14.5 %collective-permute-start.5 = (bf16[320,512]{1,0:T(8,128)(2,1)S(1)}, bf16[320,512]{1,0:T(8,128)(2,1)S(1)}, u32[]{:S(2)}, u32[]{:S(2)}) collective-permute-start(bf16[320,512]{1,0:T(8,128)(2,1)S(1)} %get-tuple-element.26), channel_id=1, source_target_pairs={{0,1},{1,2},{2,3},{3,0},{4,5},{5,6},{6,7},{7,4},{8,9},{9,10},{10,1... | collective-permute-start | bytes 983048 | tf_op jit(solution)/shard_map/ppermute | solution.py:33
  67.7 14.0 %collective-permute-start.4 = (bf16[320,512]{1,0:T(8,128)(2,1)S(1)}, bf16[320,512]{1,0:T(8,128)(2,1)S(1)}, u32[]{:S(2)}, u32[]{:S(2)}) collective-permute-start(bf16[320,512]{1,0:T(8,128)(2,1)S(1)} %add_convert_fusion.3), channel_id=1, source_target_pairs={{0,1},{1,2},{2,3},{3,0},{4,5},{5,6},{6,7},{7,4},{8,9},{9,10},{10,1... | collective-permute-start | bytes 983048 | tf_op jit(solution)/shard_map/ppermute | solution.py:33
  67.9 13.7 %collective-permute-start.7 = (bf16[320,512]{1,0:T(8,128)(2,1)S(1)}, bf16[320,512]{1,0:T(8,128)(2,1)S(1)}, u32[]{:S(2)}, u32[]{:S(2)}) collective-permute-start(bf16[320,512]{1,0:T(8,128)(2,1)S(1)} %add_convert_fusion.2), channel_id=1, source_target_pairs={{0,3},{1,0},{2,1},{3,2},{4,7},{5,4},{6,5},{7,6},{8,11},{9,8},{10,9... | collective-permute-start | bytes 983048 | tf_op jit(solution)/shard_map/ppermute | solution.py:33
  81.8 15.3 %collective-permute-start.9 = (bf16[640,512]{1,0:T(8,128)(2,1)S(1)}, bf16[640,512]{1,0:T(8,128)(2,1)S(1)}, u32[]{:S(2)}, u32[]{:S(2)}) collective-permute-start(bf16[640,512]{1,0:T(8,128)(2,1)S(1)} %settle.1.own_ref.base_ref), channel_id=1, source_target_pairs={{0,3},{1,0},{2,1},{3,2},{4,7},{5,4},{6,5},{7,6},{8,11},{9,8},{10,9... | collective-permute-start | bytes 1966088 | tf_op jit(solution)/shard_map/ppermute | solution.py:33
  84.3 16.3 %collective-permute-start.8 = (bf16[640,512]{1,0:T(8,128)(2,1)S(1)}, bf16[640,512]{1,0:T(8,128)(2,1)S(1)}, u32[]{:S(2)}, u32[]{:S(2)}) collective-permute-start(bf16[640,512]{1,0:T(8,128)(2,1)S(1)} %settle.1.own_ref.base_ref), channel_id=1, source_target_pairs={{0,1},{1,2},{2,3},{3,0},{4,5},{5,6},{6,7},{7,4},{8,9},{9,10},{10,1... | collective-permute-start | bytes 1966088 | tf_op jit(solution)/shard_map/ppermute | solution.py:33
  97.2 3.5 %copy-start = (bf16[640,512]{1,0:T(8,128)(2,1)}, bf16[640,512]{1,0:T(8,128)(2,1)S(1)}, u32[]{:S(2)}) copy-start(bf16[640,512]{1,0:T(8,128)(2,1)S(1)} %collective-permute-done.9.right_ref) | copy-start | bytes 1966084
  97.2 8.3 %collective-permute-start.11 = (bf16[320,512]{1,0:T(8,128)(2,1)S(1)}, bf16[320,512]{1,0:T(8,128)(2,1)S(1)}, u32[]{:S(2)}, u32[]{:S(2)}) collective-permute-start(bf16[320,512]{1,0:T(8,128)(2,1)S(1)} %slice.114), channel_id=1, source_target_pairs={{0,3},{1,0},{2,1},{3,2},{4,7},{5,4},{6,5},{7,6},{8,11},{9,8},{10,9... | collective-permute-start | bytes 983048 | tf_op jit(solution)/shard_map/ppermute | solution.py:33
  101.5 8.1 %collective-permute-start.10 = (bf16[320,512]{1,0:T(8,128)(2,1)S(1)}, bf16[320,512]{1,0:T(8,128)(2,1)S(1)}, u32[]{:S(2)}, u32[]{:S(2)}) collective-permute-start(bf16[320,512]{1,0:T(8,128)(2,1)S(1)} %slice.113), channel_id=1, source_target_pairs={{0,1},{1,2},{2,3},{3,0},{4,5},{5,6},{6,7},{7,4},{8,9},{9,10},{10,1... | collective-permute-start | bytes 983048 | tf_op jit(solution)/shard_map/ppermute | solution.py:33
  111.4 1.1 copy-start.3
  146.6 9.3 %collective-permute-start.16 = (bf16[320,512]{1,0:T(8,128)(2,1)S(1)}, bf16[320,512]{1,0:T(8,128)(2,1)S(1)}, u32[]{:S(2)}, u32[]{:S(2)}) collective-permute-start(bf16[320,512]{1,0:T(8,128)(2,1)S(1)} %get-tuple-element.38), channel_id=1, source_target_pairs={{0,3},{1,0},{2,1},{3,2},{4,7},{5,4},{6,5},{7,6},{8,11},{9,8},{10,9... | collective-permute-start | bytes 983048 | tf_op jit(solution)/shard_map/ppermute | solution.py:33
  149.1 18.4 %collective-permute-start.15 = (bf16[320,512]{1,0:T(8,128)(2,1)S(1)}, bf16[320,512]{1,0:T(8,128)(2,1)S(1)}, u32[]{:S(2)}, u32[]{:S(2)}) collective-permute-start(bf16[320,512]{1,0:T(8,128)(2,1)S(1)} %get-tuple-element.36), channel_id=1, source_target_pairs={{0,1},{1,2},{2,3},{3,0},{4,5},{5,6},{6,7},{7,4},{8,9},{9,10},{10,1... | collective-permute-start | bytes 983048 | tf_op jit(solution)/shard_map/ppermute | solution.py:33
  149.1 18.4 %collective-permute-start.12 = (bf16[320,512]{1,0:T(8,128)(2,1)S(1)}, bf16[320,512]{1,0:T(8,128)(2,1)S(1)}, u32[]{:S(2)}, u32[]{:S(2)}) collective-permute-start(bf16[320,512]{1,0:T(8,128)(2,1)S(1)} %get-tuple-element.33), channel_id=1, source_target_pairs={{0,3},{1,0},{2,1},{3,2},{4,7},{5,4},{6,5},{7,6},{8,11},{9,8},{10,9... | collective-permute-start | bytes 983048 | tf_op jit(solution)/shard_map/ppermute | solution.py:33
  151.8 14.3 %collective-permute-start.13 = (bf16[320,512]{1,0:T(8,128)(2,1)S(1)}, bf16[320,512]{1,0:T(8,128)(2,1)S(1)}, u32[]{:S(2)}, u32[]{:S(2)}) collective-permute-start(bf16[320,512]{1,0:T(8,128)(2,1)S(1)} %get-tuple-element.35), channel_id=1, source_target_pairs={{0,1},{1,2},{2,3},{3,0},{4,5},{5,6},{6,7},{7,4},{8,9},{9,10},{10,1... | collective-permute-start | bytes 983048 | tf_op jit(solution)/shard_map/ppermute | solution.py:33
  156.0 14.0 %collective-permute-start.17 = (bf16[320,512]{1,0:T(8,128)(2,1)S(1)}, bf16[320,512]{1,0:T(8,128)(2,1)S(1)}, u32[]{:S(2)}, u32[]{:S(2)}) collective-permute-start(bf16[320,512]{1,0:T(8,128)(2,1)S(1)} %add_convert_fusion), channel_id=1, source_target_pairs={{0,3},{1,0},{2,1},{3,2},{4,7},{5,4},{6,5},{7,6},{8,11},{9,8},{10,9... | collective-permute-start | bytes 983048 | tf_op jit(solution)/shard_map/ppermute | solution.py:33
  166.2 9.2 %collective-permute-start.14 = (bf16[320,512]{1,0:T(8,128)(2,1)S(1)}, bf16[320,512]{1,0:T(8,128)(2,1)S(1)}, u32[]{:S(2)}, u32[]{:S(2)}) collective-permute-start(bf16[320,512]{1,0:T(8,128)(2,1)S(1)} %add_convert_fusion.1), channel_id=1, source_target_pairs={{0,1},{1,2},{2,3},{3,0},{4,5},{5,6},{6,7},{7,4},{8,9},{9,10},{10,1... | collective-permute-start | bytes 983048 | tf_op jit(solution)/shard_map/ppermute | solution.py:33
  (6 other events, 5.4 us)
Sparse Core Ops, SparseCore 0:
  9.2 122.4 all-gather.1

commit v3 on v2

--- a/solution.py
+++ b/solution.py
@@ -257,11 +257,12 @@
 def low_kernel(normed_ref, both_ref, down_ref, hidden_ref, far_ref, right_ref):
     count, first = divmod(hidden_ref.shape[1], CHUNK)
     rows = hidden_ref.shape[0]
-    hide(normed_ref, both_ref, hidden_ref, rows, 0, first)
+    low = normed_ref.shape[0] - rows
+    hide(normed_ref, both_ref, hidden_ref, low, 0, first)
 
     def body(i, carry):
         at = pl.multiple_of(first + i * CHUNK, 128)
-        hide(normed_ref, both_ref, hidden_ref, rows, at, CHUNK)
+        hide(normed_ref, both_ref, hidden_ref, low, at, CHUNK)
         return carry
 
     lax.fori_loop(0, count, body, 0)
@@ -275,20 +276,21 @@
 
 def own_kernel(top_ref, low_ref, down_ref, base_ref, out_ref):
     half = top_ref.shape[0]
-    for at, hidden_ref in ((0, top_ref), (half, low_ref)):
+    for rows, hidden_ref in ((slice(None, half), top_ref), (slice(half, None), low_ref)):
         terms = times_transposed(hidden_ref[...], down_ref[3])
-        out_ref[at : at + half] = terms + base_ref[at : at + half].astype(jnp.float32)
+        out_ref[rows] = terms + base_ref[rows].astype(jnp.float32)
 
 
 def feed_forward(places, normed, weights, base, axis):
     tok, model = normed.shape
     owned = base.shape[1]
     units = weights.shape[1] // 3
-    half = tok // 2
     vmem = pl.BlockSpec(memory_space=pltpu.VMEM)
-    part, hid = ((half, owned), (half, units))
+    first = tok * 11 // 20
+    part, hid = ((first, owned), (first, units))
+    low_part, low_hid = ((tok - first, owned), (tok - first, units))
     cost = pl.CostEstimate(
-        flops=2 * tok * model * units, bytes_accessed=6 * model * units, transcendentals=half * units
+        flops=2 * tok * model * units, bytes_accessed=6 * model * units, transcendentals=tok // 2 * units
     )
     small = pl.CostEstimate(
         flops=2 * tok * units * owned, bytes_accessed=4 * tok * owned, transcendentals=0
@@ -325,7 +327,7 @@
         low_kernel,
         in_specs=[vmem] * 3,
         out_specs=[vmem] * 3,
-        out_shape=[hold(hid), hold(part), hold(part)],
+        out_shape=[hold(low_hid), hold(low_part), hold(low_part)],
         cost_estimate=cost,
         compiler_params=grant,
         name="low",
@@ -339,7 +341,7 @@
         rest_kernel,
         in_specs=[vmem] * 3,
         out_specs=[vmem] * 2,
-        out_shape=[hold(part)] * 2,
+        out_shape=[hold(part), hold(low_part)],
         cost_estimate=small,
         compiler_params=grant,
         name="rest",

time: 184 us -> 180 us (0.978)
  waiting for transfers between devices: 70 us -> 66.1 us
    ppermute x16, waiting for transfers between devices: 54.4 us -> 50.4 us  [shifted(): lax.ppermute(array, axis, [(i, (i + by) % count) for i in range(count)])]
  transfers between devices with their start and end apart: 19 -> 19, of which waited for: 12 -> 11; matrix products, arithmetic and copies ran while one was open for 11% -> 11% of each run, Pallas kernels for 4% -> 7%
where the time goes in v3:
time: 180 us; the launch traced here: 179 us
  waiting for transfers between devices  66.1 us (37%)
  starting transfers between devices  46.1 us (26%)
  Pallas kernels  23.4 us (13%)
  local copies, waits for them, and re-layouts  18.8 us (10%)
  between operations  13.9 us (8%)
  other arithmetic  6.69 us (4%)
  matrix products  4.33 us (2%)
    ppermute x16, waiting for transfers between devices, shifted(): lax.ppermute(array, axis, [(i, (i + by) % count) for i in range(count)])  50.4 us
    ppermute x1, starting transfers between devices, with_halo(): lax.ppermute(head, axis, [((i + 1) % count, i) for i in range(ends)])  22.4 us
    ppermute x16, starting transfers between devices, shifted(): lax.ppermute(array, axis, [(i, (i + by) % count) for i in range(count)])  21.8 us
    all_gather x1, waiting for transfers between devices, body(): weights = lax.all_gather(shard, 'sp', axis=0, tiled=True)  15.6 us
    unnamed x28, local copies, waits for them, and re-layouts  9.45 us
    pallas_call x1, Pallas kernels, feed_forward(): pl.pallas_call(top_kernel, in_specs=[pl.BlockSpec(memory_space=pltpu.SMEM...  8.95 us
    pallas_call x1, Pallas kernels, feed_forward(): low, far_low, right_low = low_half(normed, both, down)  5.92 us
    reshape x2, local copies, waits for them, and re-layouts, body(): attended = attended.astype(jnp.bfloat16).reshape(tok, heads_here * HEAD_DIM)  5.89 us
  transfers between devices with their start and end apart: 19, of which 11 were waited for; matrix products, arithmetic and copies ran while one was open for 11% of the time, Pallas kernels for 7%

profile of v3, /device:TPU:33, one launch (start us, length us, event | category | flops | bytes accessed | tf_op | source)
XLA Modules:
  0.0 179.2 jit_solution(16295200064532275590)
XLA Ops:
  11.2 22.4 %collective-permute-start.1 = (bf16[128,2,128]{0,2,1:T(8,128)(2,1)S(1)}, bf16[128,2,128]{0,2,1:T(8,128)(2,1)S(1)}, u32[]{:S(2)}, u32[]{:S(2)}) collective-permute-start(bf16[128,2,128]{0,2,1:T(8,128)(2,1)S(1)} %get-tuple-element.45), channel_id=1, source_target_pairs={{4,0},{8,4},{12,8},{16,12},{20,16},{24,20},{28,24},{32,28},{36,32}... | collective-permute-start | bytes 196616 | tf_op jit(solution)/shard_map/ppermute | solution.py:24
  33.6 2.0 %collective-permute-start = (bf16[128,2,128]{0,2,1:T(8,128)(2,1)S(1)}, bf16[128,2,128]{0,2,1:T(8,128)(2,1)S(1)}, u32[]{:S(2)}, u32[]{:S(2)}) collective-permute-start(bf16[128,2,128]{0,2,1:T(8,128)(2,1)S(1)} %get-tuple-element.46), channel_id=1, source_target_pairs={{0,4},{4,8},{8,12},{12,16},{16,20},{20,24},{24,28},{28,32},{32,36}... | collective-permute-start | bytes 196616 | tf_op jit(solution)/shard_map/ppermute | solution.py:22
  42.0 1.9 %fusion = f32[5,2,4,128]{3,2,1,0:T(4,128)S(1)} fusion(f32[5,2,384,128,4]{3,2,4,1,0:T(8,128)S(1)} %get-tuple-element.58, f32[5,2,4,128]{3,2,1,0:T(4,128)S(1)} %broadcast_maximum_fusion, pred[5,128,384]{1,2,0:T(8,128)(4,1)S(1)} %fusion.6), kind=kLoop, calls=%fused_computation.3 | loop fusion | flops 7859200 | bytes 8151040 | tf_op jit(solution)/shard_map/reduce_sum | solution.py:436
  44.1 3.1 %fusion.4 = bf16[5,128,2,4,64]{1,4,3,2,0:T(8,128)(2,1)} fusion(f32[5,2,384,128,4]{3,2,4,1,0:T(8,128)S(1)} %get-tuple-element.58, f32[5,2,4,128]{3,2,1,0:T(4,128)S(1)} %exponential_add_fusion, f32[5,2,4,128]{3,2,1,0:T(4,128)S(1)} %broadcast_maximum_fusion, pred[5,128,384]{1,2,0:T(8,128)(4,1)S(1)} %fusion.6, bf16[5,384,2,128]{1,3,2,0:T(8,128)(2,1)S(1)} %fusion.16), kind=kOutput, calls=%fused_computation.7 | convolution fusion | flops 261816320 | bytes 9297920 | tf_op jit(solution)/shard_map/nkgqj,njkd->nqkgd/dot_general | solution.py:438
  47.1 3.3 %copy.31 = bf16[5,128,2,4,64]{4,3,2,1,0:T(4,128)(2,1)} copy(bf16[5,128,2,4,64]{1,4,3,2,0:T(8,128)(2,1)} %fusion.4) | data formatting | bytes 1310720 | tf_op jit(solution)/shard_map/reshape | solution.py:441
  50.4 2.6 %reshape.259.rows_ref = bf16[640,512]{1,0:T(8,128)(2,1)S(1)} reshape(bf16[5,128,2,4,64]{4,3,2,1,0:T(4,128)(2,1)} %copy.31) | data formatting | bytes 1310720 | tf_op jit(solution)/shard_map/reshape | solution.py:441
  54.2 3.1 %project.1 = (bf16[320,512]{1,0:T(8,128)(2,1)S(1)}, bf16[320,512]{1,0:T(8,128)(2,1)S(1)}, bf16[320,512]{1,0:T(8,128)(2,1)S(1)}, bf16[320,512]{1,0:T(8,128)(2,1)S...) custom-call(s32[4]{0:T(128)S(1)} %pad_add_fusion.places_ref, ...), custom_call_target="tpu_custom_call" | custom-call | flops 1342177280 | bytes 6684672 | tf_op jit(solution)/shard_map/project/pallas_call | solution.py:102
  57.4 2.7 %collective-permute-start.6 = (bf16[320,512]{1,0:T(8,128)(2,1)S(1)}, bf16[320,512]{1,0:T(8,128)(2,1)S(1)}, u32[]{:S(2)}, u32[]{:S(2)}) collective-permute-start(bf16[320,512]{1,0:T(8,128)(2,1)S(1)} %get-tuple-element.28), channel_id=1, source_target_pairs={{0,3},{1,0},{2,1},{3,2},{4,7},{5,4},{6,5},{7,6},{8,11},{9,8},{10,9... | collective-permute-start | bytes 983048 | tf_op jit(solution)/shard_map/ppermute | solution.py:33
  61.6 6.0 %collective-permute-done.3 = bf16[320,512]{1,0:T(8,128)(2,1)S(1)} collective-permute-done((bf16[320,512]{1,0:T(8,128)(2,1)S(1)}, bf16[320,512]{1,0:T(8,128)(2,1)S(1)}, u32[]{:S(2)}, u32[]{:S(2)}) %collective-permute-start.3) | collective-permute-done | bytes 327712 | tf_op jit(solution)/shard_map/ppermute | solution.py:33
  67.9 2.8 %collective-permute-start.7 = (bf16[320,512]{1,0:T(8,128)(2,1)S(1)}, bf16[320,512]{1,0:T(8,128)(2,1)S(1)}, u32[]{:S(2)}, u32[]{:S(2)}) collective-permute-start(bf16[320,512]{1,0:T(8,128)(2,1)S(1)} %add_convert_fusion.1), channel_id=1, source_target_pairs={{0,3},{1,0},{2,1},{3,2},{4,7},{5,4},{6,5},{7,6},{8,11},{9,8},{10,9... | collective-permute-start | bytes 983048 | tf_op jit(solution)/shard_map/ppermute | solution.py:33
  70.7 3.0 %collective-permute-done.2.top_ref = bf16[320,512]{1,0:T(8,128)(2,1)S(1)} collective-permute-done((bf16[320,512]{1,0:T(8,128)(2,1)S(1)}, bf16[320,512]{1,0:T(8,128)(2,1)S(1)}, u32[]{:S(2)}, u32[]{:S(2)}) %collective-permute-start.2) | collective-permute-done | bytes 327712 | tf_op jit(solution)/shard_map/ppermute | solution.py:33
  74.6 7.0 %collective-permute-done.4.top2_ref = bf16[320,512]{1,0:T(8,128)(2,1)S(1)} collective-permute-done((bf16[320,512]{1,0:T(8,128)(2,1)S(1)}, bf16[320,512]{1,0:T(8,128)(2,1)S(1)}, u32[]{:S(2)}, u32[]{:S(2)}) %collective-permute-start.4) | collective-permute-done | bytes 327712 | tf_op jit(solution)/shard_map/ppermute | solution.py:33
  81.8 2.5 %collective-permute-start.9 = (bf16[640,512]{1,0:T(8,128)(2,1)S(1)}, bf16[640,512]{1,0:T(8,128)(2,1)S(1)}, u32[]{:S(2)}, u32[]{:S(2)}) collective-permute-start(bf16[640,512]{1,0:T(8,128)(2,1)S(1)} %settle.1.own_ref.base_ref), channel_id=1, source_target_pairs={{0,3},{1,0},{2,1},{3,2},{4,7},{5,4},{6,5},{7,6},{8,11},{9,8},{10,9... | collective-permute-start | bytes 1966088 | tf_op jit(solution)/shard_map/ppermute | solution.py:33
  84.3 12.8 %collective-permute-done.9.right_ref = bf16[640,512]{1,0:T(8,128)(2,1)S(1)} collective-permute-done((bf16[640,512]{1,0:T(8,128)(2,1)S(1)}, bf16[640,512]{1,0:T(8,128)(2,1)S(1)}, u32[]{:S(2)}, u32[]{:S(2)}) %collective-permute-start.9) | collective-permute-done | bytes 655392 | tf_op jit(solution)/shard_map/ppermute | solution.py:33
  97.2 3.4 %collective-permute-start.11 = (bf16[320,512]{1,0:T(8,128)(2,1)S(1)}, bf16[320,512]{1,0:T(8,128)(2,1)S(1)}, u32[]{:S(2)}, u32[]{:S(2)}) collective-permute-start(bf16[320,512]{1,0:T(8,128)(2,1)S(1)} %slice.114), channel_id=1, source_target_pairs={{0,3},{1,0},{2,1},{3,2},{4,7},{5,4},{6,5},{7,6},{8,11},{9,8},{10,9... | collective-permute-start | bytes 983048 | tf_op jit(solution)/shard_map/ppermute | solution.py:33
  101.5 4.0 %collective-permute-done.11.low_ref = bf16[320,512]{1,0:T(8,128)(2,1)S(1)} collective-permute-done((bf16[320,512]{1,0:T(8,128)(2,1)S(1)}, bf16[320,512]{1,0:T(8,128)(2,1)S(1)}, u32[]{:S(2)}, u32[]{:S(2)}) %collective-permute-start.11) | collective-permute-done | bytes 327712 | tf_op jit(solution)/shard_map/ppermute | solution.py:33
  106.2 3.3 %collective-permute-done.10.top_ref = bf16[320,512]{1,0:T(8,128)(2,1)S(1)} collective-permute-done((bf16[320,512]{1,0:T(8,128)(2,1)S(1)}, bf16[320,512]{1,0:T(8,128)(2,1)S(1)}, u32[]{:S(2)}, u32[]{:S(2)}) %collective-permute-start.10) | collective-permute-done | bytes 327712 | tf_op jit(solution)/shard_map/ppermute | solution.py:33
  116.1 15.6 %all-gather.2.cloned.1.call-done.weights_ref = bf16[2048,4224]{1,0:T(8,128)(2,1)} async-done(((bf16[64,4224]{1,0:T(8,128)(2,1)}), bf16[2048,4224]{1,0:T(8,128)(2,1)}) %all-gather.2.cloned.1.call-update) | async-done | bytes 17301520 | tf_op jit(solution)/shard_map/all_gather | solution.py:400
  131.7 9.0 %top.1 = (bf16[352,1408]{1,0:T(8,128)(2,1)S(1)}, bf16[352,512]{1,0:T(8,128)(2,1)S(1)}, bf16[352,512]{1,0:T(8,128)(2,1)S(1)}, bf16[2048,2816]{1,0:T(8,128)(2,1)S(1)}, bf16[4,512,1408]{2,1,0:T(8,128)(2,1)S(1)}) custom-call(s32[4]{0:T(128)S(1)} %pad_add_fusion.places_ref, bf16[640,2048]{1,0:T(8,128)(2,1)S(1)} %norm.1.normed_ref, ...), custom_call_target="tpu_custom_call" | custom-call | flops 3690987520 | bytes 17301504 | tf_op jit(solution)/shard_map/top/pallas_call | solution.py:300
  142.2 5.9 %low.1 = (bf16[288,1408]{1,0:T(8,128)(2,1)S(1)}, bf16[288,512]{1,0:T(8,128)(2,1)S(1)}, bf16[288,512]{1,0:T(8,128)(2,1)S(1)}) custom-call(bf16[640,2048]{1,0:T(8,128)(2,1)S(1)} %norm.1.normed_ref, bf16[2048,2816]{1,0:T(8,128)(2,1)S(1)} %get-tuple-element.30.both_ref, bf16[4,512,1408]{2,1,0:T(8,128)(2,1)S(1)} %get-tuple-element.31.down_ref), custom_call_target="tpu_custom_call" | custom-call | flops 3690987520 | bytes 17301504 | tf_op jit(solution)/shard_map/low/pallas_call | solution.py:336
  153.8 3.4 %collective-permute-done.16 = bf16[288,512]{1,0:T(8,128)(2,1)S(1)} collective-permute-done((bf16[288,512]{1,0:T(8,128)(2,1)S(1)}, bf16[288,512]{1,0:T(8,128)(2,1)S(1)}, u32[]{:S(2)}, u32[]{:S(2)}) %collective-permute-start.16) | collective-permute-done | bytes 294944 | tf_op jit(solution)/shard_map/ppermute | solution.py:33
  157.3 2.8 %collective-permute-start.17 = (bf16[288,512]{1,0:T(8,128)(2,1)S(1)}, bf16[288,512]{1,0:T(8,128)(2,1)S(1)}, u32[]{:S(2)}, u32[]{:S(2)}) collective-permute-start(bf16[288,512]{1,0:T(8,128)(2,1)S(1)} %add_convert_fusion.3), channel_id=1, source_target_pairs={{0,3},{1,0},{2,1},{3,2},{4,7},{5,4},{6,5},{7,6},{8,11},{9,8},{10,9... | collective-permute-start | bytes 884744 | tf_op jit(solution)/shard_map/ppermute | solution.py:33
  161.3 3.6 %collective-permute-done.12.top_ref = bf16[352,512]{1,0:T(8,128)(2,1)S(1)} collective-permute-done((bf16[352,512]{1,0:T(8,128)(2,1)S(1)}, bf16[352,512]{1,0:T(8,128)(2,1)S(1)}, u32[]{:S(2)}, u32[]{:S(2)}) %collective-permute-start.12) | collective-permute-done | bytes 360480 | tf_op jit(solution)/shard_map/ppermute | solution.py:33
  164.9 6.3 %collective-permute-done.17.low2_ref = bf16[288,512]{1,0:T(8,128)(2,1)S(1)} collective-permute-done((bf16[288,512]{1,0:T(8,128)(2,1)S(1)}, bf16[288,512]{1,0:T(8,128)(2,1)S(1)}, u32[]{:S(2)}, u32[]{:S(2)}) %collective-permute-start.17) | collective-permute-done | bytes 294944 | tf_op jit(solution)/shard_map/ppermute | solution.py:33
  (96 shorter events, 32.9 us)
Async XLA Ops:
  6.5 125.2 %all-gather.2.cloned.1.call-start = ((), (), s32[]{:S(2)}) async-start(), calls=%async_computation | async-start | bytes 17842176 | tf_op jit(solution)/shard_map/all_gather | solution.py:400
  11.2 29.4 %collective-permute-start.1 = (bf16[128,2,128]{0,2,1:T(8,128)(2,1)S(1)}, bf16[128,2,128]{0,2,1:T(8,128)(2,1)S(1)}, u32[]{:S(2)}, u32[]{:S(2)}) collective-permute-start(bf16[128,2,128]{0,2,1:T(8,128)(2,1)S(1)} %get-tuple-element.45), channel_id=1, source_target_pairs={{4,0},{8,4},{12,8},{16,12},{20,16},{24,20},{28,24},{32,28},{36,32}... | collective-permute-start | bytes 196616 | tf_op jit(solution)/shard_map/ppermute | solution.py:24
  33.6 6.9 %collective-permute-start = (bf16[128,2,128]{0,2,1:T(8,128)(2,1)S(1)}, bf16[128,2,128]{0,2,1:T(8,128)(2,1)S(1)}, u32[]{:S(2)}, u32[]{:S(2)}) collective-permute-start(bf16[128,2,128]{0,2,1:T(8,128)(2,1)S(1)} %get-tuple-element.46), channel_id=1, source_target_pairs={{0,4},{4,8},{8,12},{12,16},{16,20},{20,24},{24,28},{28,32},{32,36}... | collective-permute-start | bytes 196616 | tf_op jit(solution)/shard_map/ppermute | solution.py:22
  44.0 9.0 %copy-start.8 = (bf16[512,2048]{1,0:T(8,128)(2,1)S(1)}, bf16[512,2048]{1,0:T(8,128)(2,1)}, u32[]{:S(2)}) copy-start(bf16[512,2048]{1,0:T(8,128)(2,1)} %weight_ref.1) | copy-start | bytes 6291460
  47.1 54.3 %copy-start.10 = (f32[2048]{0:T(1024)S(1)}, f32[2048]{0:T(1024)}, u32[]{:S(2)}) copy-start(f32[2048]{0:T(1024)} %param.14) | copy-start | bytes 24580
  53.0 1.1 copy-start.9
  57.3 10.3 %collective-permute-start.3 = (bf16[320,512]{1,0:T(8,128)(2,1)S(1)}, bf16[320,512]{1,0:T(8,128)(2,1)S(1)}, u32[]{:S(2)}, u32[]{:S(2)}) collective-permute-start(bf16[320,512]{1,0:T(8,128)(2,1)S(1)} %get-tuple-element.25), channel_id=1, source_target_pairs={{0,1},{1,2},{2,3},{3,0},{4,5},{5,6},{6,7},{7,4},{8,9},{9,10},{10,1... | collective-permute-start | bytes 983048 | tf_op jit(solution)/shard_map/ppermute | solution.py:33
  57.4 10.4 %collective-permute-start.6 = (bf16[320,512]{1,0:T(8,128)(2,1)S(1)}, bf16[320,512]{1,0:T(8,128)(2,1)S(1)}, u32[]{:S(2)}, u32[]{:S(2)}) collective-permute-start(bf16[320,512]{1,0:T(8,128)(2,1)S(1)} %get-tuple-element.28), channel_id=1, source_target_pairs={{0,3},{1,0},{2,1},{3,2},{4,7},{5,4},{6,5},{7,6},{8,11},{9,8},{10,9... | collective-permute-start | bytes 983048 | tf_op jit(solution)/shard_map/ppermute | solution.py:33
  60.1 13.6 %collective-permute-start.2 = (bf16[320,512]{1,0:T(8,128)(2,1)S(1)}, bf16[320,512]{1,0:T(8,128)(2,1)S(1)}, u32[]{:S(2)}, u32[]{:S(2)}) collective-permute-start(bf16[320,512]{1,0:T(8,128)(2,1)S(1)} %get-tuple-element.23), channel_id=1, source_target_pairs={{0,3},{1,0},{2,1},{3,2},{4,7},{5,4},{6,5},{7,6},{8,11},{9,8},{10,9... | collective-permute-start | bytes 983048 | tf_op jit(solution)/shard_map/ppermute | solution.py:33
  60.1 14.5 %collective-permute-start.5 = (bf16[320,512]{1,0:T(8,128)(2,1)S(1)}, bf16[320,512]{1,0:T(8,128)(2,1)S(1)}, u32[]{:S(2)}, u32[]{:S(2)}) collective-permute-start(bf16[320,512]{1,0:T(8,128)(2,1)S(1)} %get-tuple-element.26), channel_id=1, source_target_pairs={{0,1},{1,2},{2,3},{3,0},{4,5},{5,6},{6,7},{7,4},{8,9},{9,10},{10,1... | collective-permute-start | bytes 983048 | tf_op jit(solution)/shard_map/ppermute | solution.py:33
  67.7 14.0 %collective-permute-start.4 = (bf16[320,512]{1,0:T(8,128)(2,1)S(1)}, bf16[320,512]{1,0:T(8,128)(2,1)S(1)}, u32[]{:S(2)}, u32[]{:S(2)}) collective-permute-start(bf16[320,512]{1,0:T(8,128)(2,1)S(1)} %add_convert_fusion.2), channel_id=1, source_target_pairs={{0,1},{1,2},{2,3},{3,0},{4,5},{5,6},{6,7},{7,4},{8,9},{9,10},{10,1... | collective-permute-start | bytes 983048 | tf_op jit(solution)/shard_map/ppermute | solution.py:33
  67.9 13.7 %collective-permute-start.7 = (bf16[320,512]{1,0:T(8,128)(2,1)S(1)}, bf16[320,512]{1,0:T(8,128)(2,1)S(1)}, u32[]{:S(2)}, u32[]{:S(2)}) collective-permute-start(bf16[320,512]{1,0:T(8,128)(2,1)S(1)} %add_convert_fusion.1), channel_id=1, source_target_pairs={{0,3},{1,0},{2,1},{3,2},{4,7},{5,4},{6,5},{7,6},{8,11},{9,8},{10,9... | collective-permute-start | bytes 983048 | tf_op jit(solution)/shard_map/ppermute | solution.py:33
  81.8 15.3 %collective-permute-start.9 = (bf16[640,512]{1,0:T(8,128)(2,1)S(1)}, bf16[640,512]{1,0:T(8,128)(2,1)S(1)}, u32[]{:S(2)}, u32[]{:S(2)}) collective-permute-start(bf16[640,512]{1,0:T(8,128)(2,1)S(1)} %settle.1.own_ref.base_ref), channel_id=1, source_target_pairs={{0,3},{1,0},{2,1},{3,2},{4,7},{5,4},{6,5},{7,6},{8,11},{9,8},{10,9... | collective-permute-start | bytes 1966088 | tf_op jit(solution)/shard_map/ppermute | solution.py:33
  84.3 16.3 %collective-permute-start.8 = (bf16[640,512]{1,0:T(8,128)(2,1)S(1)}, bf16[640,512]{1,0:T(8,128)(2,1)S(1)}, u32[]{:S(2)}, u32[]{:S(2)}) collective-permute-start(bf16[640,512]{1,0:T(8,128)(2,1)S(1)} %settle.1.own_ref.base_ref), channel_id=1, source_target_pairs={{0,1},{1,2},{2,3},{3,0},{4,5},{5,6},{6,7},{7,4},{8,9},{9,10},{10,1... | collective-permute-start | bytes 1966088 | tf_op jit(solution)/shard_map/ppermute | solution.py:33
  97.2 3.5 %copy-start = (bf16[640,512]{1,0:T(8,128)(2,1)}, bf16[640,512]{1,0:T(8,128)(2,1)S(1)}, u32[]{:S(2)}) copy-start(bf16[640,512]{1,0:T(8,128)(2,1)S(1)} %collective-permute-done.9.right_ref) | copy-start | bytes 1966084
  97.2 8.3 %collective-permute-start.11 = (bf16[320,512]{1,0:T(8,128)(2,1)S(1)}, bf16[320,512]{1,0:T(8,128)(2,1)S(1)}, u32[]{:S(2)}, u32[]{:S(2)}) collective-permute-start(bf16[320,512]{1,0:T(8,128)(2,1)S(1)} %slice.114), channel_id=1, source_target_pairs={{0,3},{1,0},{2,1},{3,2},{4,7},{5,4},{6,5},{7,6},{8,11},{9,8},{10,9... | collective-permute-start | bytes 983048 | tf_op jit(solution)/shard_map/ppermute | solution.py:33
  101.5 8.1 %collective-permute-start.10 = (bf16[320,512]{1,0:T(8,128)(2,1)S(1)}, bf16[320,512]{1,0:T(8,128)(2,1)S(1)}, u32[]{:S(2)}, u32[]{:S(2)}) collective-permute-start(bf16[320,512]{1,0:T(8,128)(2,1)S(1)} %slice.113), channel_id=1, source_target_pairs={{0,1},{1,2},{2,3},{3,0},{4,5},{5,6},{6,7},{7,4},{8,9},{9,10},{10,1... | collective-permute-start | bytes 983048 | tf_op jit(solution)/shard_map/ppermute | solution.py:33
  111.4 1.1 copy-start.3
  140.7 11.7 %collective-permute-start.13 = (bf16[352,512]{1,0:T(8,128)(2,1)S(1)}, bf16[352,512]{1,0:T(8,128)(2,1)S(1)}, u32[]{:S(2)}, u32[]{:S(2)}) collective-permute-start(bf16[352,512]{1,0:T(8,128)(2,1)S(1)} %get-tuple-element.35), channel_id=1, source_target_pairs={{0,1},{1,2},{2,3},{3,0},{4,5},{5,6},{6,7},{7,4},{8,9},{9,10},{10,1... | collective-permute-start | bytes 1081352 | tf_op jit(solution)/shard_map/ppermute | solution.py:33
  148.1 13.1 %collective-permute-start.15 = (bf16[288,512]{1,0:T(8,128)(2,1)S(1)}, bf16[288,512]{1,0:T(8,128)(2,1)S(1)}, u32[]{:S(2)}, u32[]{:S(2)}) collective-permute-start(bf16[288,512]{1,0:T(8,128)(2,1)S(1)} %get-tuple-element.36), channel_id=1, source_target_pairs={{0,1},{1,2},{2,3},{3,0},{4,5},{5,6},{6,7},{7,4},{8,9},{9,10},{10,1... | collective-permute-start | bytes 884744 | tf_op jit(solution)/shard_map/ppermute | solution.py:33
  149.4 7.7 %collective-permute-start.16 = (bf16[288,512]{1,0:T(8,128)(2,1)S(1)}, bf16[288,512]{1,0:T(8,128)(2,1)S(1)}, u32[]{:S(2)}, u32[]{:S(2)}) collective-permute-start(bf16[288,512]{1,0:T(8,128)(2,1)S(1)} %get-tuple-element.38), channel_id=1, source_target_pairs={{0,3},{1,0},{2,1},{3,2},{4,7},{5,4},{6,5},{7,6},{8,11},{9,8},{10,9... | collective-permute-start | bytes 884744 | tf_op jit(solution)/shard_map/ppermute | solution.py:33
  150.9 14.0 %collective-permute-start.12 = (bf16[352,512]{1,0:T(8,128)(2,1)S(1)}, bf16[352,512]{1,0:T(8,128)(2,1)S(1)}, u32[]{:S(2)}, u32[]{:S(2)}) collective-permute-start(bf16[352,512]{1,0:T(8,128)(2,1)S(1)} %get-tuple-element.33), channel_id=1, source_target_pairs={{0,3},{1,0},{2,1},{3,2},{4,7},{5,4},{6,5},{7,6},{8,11},{9,8},{10,9... | collective-permute-start | bytes 1081352 | tf_op jit(solution)/shard_map/ppermute | solution.py:33
  152.5 18.7 %collective-permute-start.14 = (bf16[352,512]{1,0:T(8,128)(2,1)S(1)}, bf16[352,512]{1,0:T(8,128)(2,1)S(1)}, u32[]{:S(2)}, u32[]{:S(2)}) collective-permute-start(bf16[352,512]{1,0:T(8,128)(2,1)S(1)} %add_convert_fusion), channel_id=1, source_target_pairs={{0,1},{1,2},{2,3},{3,0},{4,5},{5,6},{6,7},{7,4},{8,9},{9,10},{10,1... | collective-permute-start | bytes 1081352 | tf_op jit(solution)/shard_map/ppermute | solution.py:33
  157.3 14.0 %collective-permute-start.17 = (bf16[288,512]{1,0:T(8,128)(2,1)S(1)}, bf16[288,512]{1,0:T(8,128)(2,1)S(1)}, u32[]{:S(2)}, u32[]{:S(2)}) collective-permute-start(bf16[288,512]{1,0:T(8,128)(2,1)S(1)} %add_convert_fusion.3), channel_id=1, source_target_pairs={{0,3},{1,0},{2,1},{3,2},{4,7},{5,4},{6,5},{7,6},{8,11},{9,8},{10,9... | collective-permute-start | bytes 884744 | tf_op jit(solution)/shard_map/ppermute | solution.py:33
  (6 other events, 5.4 us)
Sparse Core Ops, SparseCore 0:
  9.2 122.4 all-gather.1

commit v4 on v3

--- a/solution.py
+++ b/solution.py
@@ -178,6 +178,7 @@
 
 
 CHUNK = 256
+BLOCKS = 4
 
 
 def hide(normed_ref, both_ref, hidden_ref, low, at, size):
@@ -210,16 +211,18 @@
     hidden_ref, far_ref, left_ref, both_ref, down_ref, sems, down_sems = rest
     units = hidden_ref.shape[1]
     owned = far_ref.shape[1]
+    deep = both_ref.shape[0] // BLOCKS
     count, first = divmod(units, CHUNK)
 
     def copies(slot, at, size):
         return [
             pltpu.make_async_copy(
-                weights_ref.at[:, pl.ds(k * units + at, size)],
-                both_ref.at[:, pl.ds(2 * at + k * size, size)],
-                sems.at[slot, k],
+                weights_ref.at[pl.ds(block * deep, deep), pl.ds(k * units + at, size)],
+                both_ref.at[pl.ds(block * deep, deep), pl.ds(2 * at + k * size, size)],
+                sems.at[slot, k, block],
             )
             for k in range(2)
+            for block in range(BLOCKS)
         ]
 
     def down_copy(k):
@@ -313,7 +316,7 @@
             hold((4, owned, units)),
         ],
         scratch_shapes=[
-            pltpu.SemaphoreType.DMA((1 + units // CHUNK, 2)),
+            pltpu.SemaphoreType.DMA((1 + units // CHUNK, 2, BLOCKS)),
             pltpu.SemaphoreType.DMA((4,)),
         ],
         cost_estimate=cost,

time: 180 us -> 180 us (level)
  no operation moved by 1% of the time
where the time goes in v4:
time: 180 us
  waiting for transfers between devices  66 us (37%)
  starting transfers between devices  46.1 us (26%)
  Pallas kernels  23.8 us (13%)
  local copies, waits for them, and re-layouts  18.8 us (10%)
  between operations  13.9 us (8%)
  other arithmetic  6.69 us (4%)
  matrix products  4.33 us (2%)
    ppermute x16, waiting for transfers between devices, shifted(): lax.ppermute(array, axis, [(i, (i + by) % count) for i in range(count)])  50.4 us
    ppermute x1, starting transfers between devices, with_halo(): lax.ppermute(head, axis, [((i + 1) % count, i) for i in range(ends)])  22.4 us
    ppermute x16, starting transfers between devices, shifted(): lax.ppermute(array, axis, [(i, (i + by) % count) for i in range(count)])  21.8 us
    all_gather x1, waiting for transfers between devices, body(): weights = lax.all_gather(shard, 'sp', axis=0, tiled=True)  15.6 us
    unnamed x28, local copies, waits for them, and re-layouts  9.45 us
    pallas_call x1, Pallas kernels, feed_forward(): pl.pallas_call(top_kernel, in_specs=[pl.BlockSpec(memory_space=pltpu.SMEM...  9.38 us
    pallas_call x1, Pallas kernels, feed_forward(): low, far_low, right_low = low_half(normed, both, down)  5.92 us
    reshape x2, local copies, waits for them, and re-layouts, body(): attended = attended.astype(jnp.bfloat16).reshape(tok, heads_here * HEAD_DIM)  5.89 us
  transfers between devices with their start and end apart: 19, of which 11 were waited for; matrix products, arithmetic and copies ran while one was open for 11% of the time, Pallas kernels for 7%

profile of v4, /device:TPU:33, one launch (start us, length us, event | category | flops | bytes accessed | tf_op | source)
XLA Modules:
  0.0 179.6 jit_solution(6790896737426102025)
XLA Ops:
  11.2 22.4 %collective-permute-start.1 = (bf16[128,2,128]{0,2,1:T(8,128)(2,1)S(1)}, bf16[128,2,128]{0,2,1:T(8,128)(2,1)S(1)}, u32[]{:S(2)}, u32[]{:S(2)}) collective-permute-start(bf16[128,2,128]{0,2,1:T(8,128)(2,1)S(1)} %get-tuple-element.45), channel_id=1, source_target_pairs={{4,0},{8,4},{12,8},{16,12},{20,16},{24,20},{28,24},{32,28},{36,32}... | collective-permute-start | bytes 196616 | tf_op jit(solution)/shard_map/ppermute | solution.py:24
  33.6 2.0 %collective-permute-start = (bf16[128,2,128]{0,2,1:T(8,128)(2,1)S(1)}, bf16[128,2,128]{0,2,1:T(8,128)(2,1)S(1)}, u32[]{:S(2)}, u32[]{:S(2)}) collective-permute-start(bf16[128,2,128]{0,2,1:T(8,128)(2,1)S(1)} %get-tuple-element.46), channel_id=1, source_target_pairs={{0,4},{4,8},{8,12},{12,16},{16,20},{20,24},{24,28},{28,32},{32,36}... | collective-permute-start | bytes 196616 | tf_op jit(solution)/shard_map/ppermute | solution.py:22
  42.0 1.9 %fusion = f32[5,2,4,128]{3,2,1,0:T(4,128)S(1)} fusion(f32[5,2,384,128,4]{3,2,4,1,0:T(8,128)S(1)} %get-tuple-element.58, f32[5,2,4,128]{3,2,1,0:T(4,128)S(1)} %broadcast_maximum_fusion, pred[5,128,384]{1,2,0:T(8,128)(4,1)S(1)} %fusion.6), kind=kLoop, calls=%fused_computation.3 | loop fusion | flops 7859200 | bytes 8151040 | tf_op jit(solution)/shard_map/reduce_sum | solution.py:439
  44.1 3.1 %fusion.4 = bf16[5,128,2,4,64]{1,4,3,2,0:T(8,128)(2,1)} fusion(f32[5,2,384,128,4]{3,2,4,1,0:T(8,128)S(1)} %get-tuple-element.58, f32[5,2,4,128]{3,2,1,0:T(4,128)S(1)} %exponential_add_fusion, f32[5,2,4,128]{3,2,1,0:T(4,128)S(1)} %broadcast_maximum_fusion, pred[5,128,384]{1,2,0:T(8,128)(4,1)S(1)} %fusion.6, bf16[5,384,2,128]{1,3,2,0:T(8,128)(2,1)S(1)} %fusion.16), kind=kOutput, calls=%fused_computation.7 | convolution fusion | flops 261816320 | bytes 9297920 | tf_op jit(solution)/shard_map/nkgqj,njkd->nqkgd/dot_general | solution.py:441
  47.1 3.3 %copy.31 = bf16[5,128,2,4,64]{4,3,2,1,0:T(4,128)(2,1)} copy(bf16[5,128,2,4,64]{1,4,3,2,0:T(8,128)(2,1)} %fusion.4) | data formatting | bytes 1310720 | tf_op jit(solution)/shard_map/reshape | solution.py:444
  50.4 2.6 %reshape.259.rows_ref = bf16[640,512]{1,0:T(8,128)(2,1)S(1)} reshape(bf16[5,128,2,4,64]{4,3,2,1,0:T(4,128)(2,1)} %copy.31) | data formatting | bytes 1310720 | tf_op jit(solution)/shard_map/reshape | solution.py:444
  54.2 3.1 %project.1 = (bf16[320,512]{1,0:T(8,128)(2,1)S(1)}, bf16[320,512]{1,0:T(8,128)(2,1)S(1)}, bf16[320,512]{1,0:T(8,128)(2,1)S(1)}, bf16[320,512]{1,0:T(8,128)(2,1)S...) custom-call(s32[4]{0:T(128)S(1)} %pad_add_fusion.places_ref, ...), custom_call_target="tpu_custom_call" | custom-call | flops 1342177280 | bytes 6684672 | tf_op jit(solution)/shard_map/project/pallas_call | solution.py:102
  57.4 2.7 %collective-permute-start.6 = (bf16[320,512]{1,0:T(8,128)(2,1)S(1)}, bf16[320,512]{1,0:T(8,128)(2,1)S(1)}, u32[]{:S(2)}, u32[]{:S(2)}) collective-permute-start(bf16[320,512]{1,0:T(8,128)(2,1)S(1)} %get-tuple-element.28), channel_id=1, source_target_pairs={{0,3},{1,0},{2,1},{3,2},{4,7},{5,4},{6,5},{7,6},{8,11},{9,8},{10,9... | collective-permute-start | bytes 983048 | tf_op jit(solution)/shard_map/ppermute | solution.py:33
  61.6 6.0 %collective-permute-done.3 = bf16[320,512]{1,0:T(8,128)(2,1)S(1)} collective-permute-done((bf16[320,512]{1,0:T(8,128)(2,1)S(1)}, bf16[320,512]{1,0:T(8,128)(2,1)S(1)}, u32[]{:S(2)}, u32[]{:S(2)}) %collective-permute-start.3) | collective-permute-done | bytes 327712 | tf_op jit(solution)/shard_map/ppermute | solution.py:33
  67.9 2.8 %collective-permute-start.7 = (bf16[320,512]{1,0:T(8,128)(2,1)S(1)}, bf16[320,512]{1,0:T(8,128)(2,1)S(1)}, u32[]{:S(2)}, u32[]{:S(2)}) collective-permute-start(bf16[320,512]{1,0:T(8,128)(2,1)S(1)} %add_convert_fusion.1), channel_id=1, source_target_pairs={{0,3},{1,0},{2,1},{3,2},{4,7},{5,4},{6,5},{7,6},{8,11},{9,8},{10,9... | collective-permute-start | bytes 983048 | tf_op jit(solution)/shard_map/ppermute | solution.py:33
  70.7 3.0 %collective-permute-done.2.top_ref = bf16[320,512]{1,0:T(8,128)(2,1)S(1)} collective-permute-done((bf16[320,512]{1,0:T(8,128)(2,1)S(1)}, bf16[320,512]{1,0:T(8,128)(2,1)S(1)}, u32[]{:S(2)}, u32[]{:S(2)}) %collective-permute-start.2) | collective-permute-done | bytes 327712 | tf_op jit(solution)/shard_map/ppermute | solution.py:33
  74.6 7.0 %collective-permute-done.4.top2_ref = bf16[320,512]{1,0:T(8,128)(2,1)S(1)} collective-permute-done((bf16[320,512]{1,0:T(8,128)(2,1)S(1)}, bf16[320,512]{1,0:T(8,128)(2,1)S(1)}, u32[]{:S(2)}, u32[]{:S(2)}) %collective-permute-start.4) | collective-permute-done | bytes 327712 | tf_op jit(solution)/shard_map/ppermute | solution.py:33
  81.8 2.5 %collective-permute-start.9 = (bf16[640,512]{1,0:T(8,128)(2,1)S(1)}, bf16[640,512]{1,0:T(8,128)(2,1)S(1)}, u32[]{:S(2)}, u32[]{:S(2)}) collective-permute-start(bf16[640,512]{1,0:T(8,128)(2,1)S(1)} %settle.1.own_ref.base_ref), channel_id=1, source_target_pairs={{0,3},{1,0},{2,1},{3,2},{4,7},{5,4},{6,5},{7,6},{8,11},{9,8},{10,9... | collective-permute-start | bytes 1966088 | tf_op jit(solution)/shard_map/ppermute | solution.py:33
  84.3 12.8 %collective-permute-done.9.right_ref = bf16[640,512]{1,0:T(8,128)(2,1)S(1)} collective-permute-done((bf16[640,512]{1,0:T(8,128)(2,1)S(1)}, bf16[640,512]{1,0:T(8,128)(2,1)S(1)}, u32[]{:S(2)}, u32[]{:S(2)}) %collective-permute-start.9) | collective-permute-done | bytes 655392 | tf_op jit(solution)/shard_map/ppermute | solution.py:33
  97.2 3.4 %collective-permute-start.11 = (bf16[320,512]{1,0:T(8,128)(2,1)S(1)}, bf16[320,512]{1,0:T(8,128)(2,1)S(1)}, u32[]{:S(2)}, u32[]{:S(2)}) collective-permute-start(bf16[320,512]{1,0:T(8,128)(2,1)S(1)} %slice.114), channel_id=1, source_target_pairs={{0,3},{1,0},{2,1},{3,2},{4,7},{5,4},{6,5},{7,6},{8,11},{9,8},{10,9... | collective-permute-start | bytes 983048 | tf_op jit(solution)/shard_map/ppermute | solution.py:33
  101.5 4.0 %collective-permute-done.11.low_ref = bf16[320,512]{1,0:T(8,128)(2,1)S(1)} collective-permute-done((bf16[320,512]{1,0:T(8,128)(2,1)S(1)}, bf16[320,512]{1,0:T(8,128)(2,1)S(1)}, u32[]{:S(2)}, u32[]{:S(2)}) %collective-permute-start.11) | collective-permute-done | bytes 327712 | tf_op jit(solution)/shard_map/ppermute | solution.py:33
  106.2 3.3 %collective-permute-done.10.top_ref = bf16[320,512]{1,0:T(8,128)(2,1)S(1)} collective-permute-done((bf16[320,512]{1,0:T(8,128)(2,1)S(1)}, bf16[320,512]{1,0:T(8,128)(2,1)S(1)}, u32[]{:S(2)}, u32[]{:S(2)}) %collective-permute-start.10) | collective-permute-done | bytes 327712 | tf_op jit(solution)/shard_map/ppermute | solution.py:33
  116.1 15.6 %all-gather.2.cloned.1.call-done.weights_ref = bf16[2048,4224]{1,0:T(8,128)(2,1)} async-done(((bf16[64,4224]{1,0:T(8,128)(2,1)}), bf16[2048,4224]{1,0:T(8,128)(2,1)}) %all-gather.2.cloned.1.call-update) | async-done | bytes 17301520 | tf_op jit(solution)/shard_map/all_gather | solution.py:403
  131.7 9.4 %top.1 = (bf16[352,1408]{1,0:T(8,128)(2,1)S(1)}, bf16[352,512]{1,0:T(8,128)(2,1)S(1)}, bf16[352,512]{1,0:T(8,128)(2,1)S(1)}, bf16[2048,2816]{1,0:T(8,128)(2,1)S(1)}, bf16[4,512,1408]{2,1,0:T(8,128)(2,1)S(1)}) custom-call(s32[4]{0:T(128)S(1)} %pad_add_fusion.places_ref, bf16[640,2048]{1,0:T(8,128)(2,1)S(1)} %norm.1.normed_ref, ...), custom_call_target="tpu_custom_call" | custom-call | flops 3690987520 | bytes 17301504 | tf_op jit(solution)/shard_map/top/pallas_call | solution.py:303
  142.6 5.9 %low.1 = (bf16[288,1408]{1,0:T(8,128)(2,1)S(1)}, bf16[288,512]{1,0:T(8,128)(2,1)S(1)}, bf16[288,512]{1,0:T(8,128)(2,1)S(1)}) custom-call(bf16[640,2048]{1,0:T(8,128)(2,1)S(1)} %norm.1.normed_ref, bf16[2048,2816]{1,0:T(8,128)(2,1)S(1)} %get-tuple-element.30.both_ref, bf16[4,512,1408]{2,1,0:T(8,128)(2,1)S(1)} %get-tuple-element.31.down_ref), custom_call_target="tpu_custom_call" | custom-call | flops 3690987520 | bytes 17301504 | tf_op jit(solution)/shard_map/low/pallas_call | solution.py:339
  154.3 3.3 %collective-permute-done.16 = bf16[288,512]{1,0:T(8,128)(2,1)S(1)} collective-permute-done((bf16[288,512]{1,0:T(8,128)(2,1)S(1)}, bf16[288,512]{1,0:T(8,128)(2,1)S(1)}, u32[]{:S(2)}, u32[]{:S(2)}) %collective-permute-start.16) | collective-permute-done | bytes 294944 | tf_op jit(solution)/shard_map/ppermute | solution.py:33
  157.7 2.8 %collective-permute-start.17 = (bf16[288,512]{1,0:T(8,128)(2,1)S(1)}, bf16[288,512]{1,0:T(8,128)(2,1)S(1)}, u32[]{:S(2)}, u32[]{:S(2)}) collective-permute-start(bf16[288,512]{1,0:T(8,128)(2,1)S(1)} %add_convert_fusion.3), channel_id=1, source_target_pairs={{0,3},{1,0},{2,1},{3,2},{4,7},{5,4},{6,5},{7,6},{8,11},{9,8},{10,9... | collective-permute-start | bytes 884744 | tf_op jit(solution)/shard_map/ppermute | solution.py:33
  161.7 3.6 %collective-permute-done.12.top_ref = bf16[352,512]{1,0:T(8,128)(2,1)S(1)} collective-permute-done((bf16[352,512]{1,0:T(8,128)(2,1)S(1)}, bf16[352,512]{1,0:T(8,128)(2,1)S(1)}, u32[]{:S(2)}, u32[]{:S(2)}) %collective-permute-start.12) | collective-permute-done | bytes 360480 | tf_op jit(solution)/shard_map/ppermute | solution.py:33
  165.3 6.3 %collective-permute-done.17.low2_ref = bf16[288,512]{1,0:T(8,128)(2,1)S(1)} collective-permute-done((bf16[288,512]{1,0:T(8,128)(2,1)S(1)}, bf16[288,512]{1,0:T(8,128)(2,1)S(1)}, u32[]{:S(2)}, u32[]{:S(2)}) %collective-permute-start.17) | collective-permute-done | bytes 294944 | tf_op jit(solution)/shard_map/ppermute | solution.py:33
  (96 shorter events, 32.8 us)
Async XLA Ops:
  6.5 125.2 %all-gather.2.cloned.1.call-start = ((), (), s32[]{:S(2)}) async-start(), calls=%async_computation | async-start | bytes 17842176 | tf_op jit(solution)/shard_map/all_gather | solution.py:403
  11.2 29.4 %collective-permute-start.1 = (bf16[128,2,128]{0,2,1:T(8,128)(2,1)S(1)}, bf16[128,2,128]{0,2,1:T(8,128)(2,1)S(1)}, u32[]{:S(2)}, u32[]{:S(2)}) collective-permute-start(bf16[128,2,128]{0,2,1:T(8,128)(2,1)S(1)} %get-tuple-element.45), channel_id=1, source_target_pairs={{4,0},{8,4},{12,8},{16,12},{20,16},{24,20},{28,24},{32,28},{36,32}... | collective-permute-start | bytes 196616 | tf_op jit(solution)/shard_map/ppermute | solution.py:24
  33.6 6.9 %collective-permute-start = (bf16[128,2,128]{0,2,1:T(8,128)(2,1)S(1)}, bf16[128,2,128]{0,2,1:T(8,128)(2,1)S(1)}, u32[]{:S(2)}, u32[]{:S(2)}) collective-permute-start(bf16[128,2,128]{0,2,1:T(8,128)(2,1)S(1)} %get-tuple-element.46), channel_id=1, source_target_pairs={{0,4},{4,8},{8,12},{12,16},{16,20},{20,24},{24,28},{28,32},{32,36}... | collective-permute-start | bytes 196616 | tf_op jit(solution)/shard_map/ppermute | solution.py:22
  44.0 9.0 %copy-start.8 = (bf16[512,2048]{1,0:T(8,128)(2,1)S(1)}, bf16[512,2048]{1,0:T(8,128)(2,1)}, u32[]{:S(2)}) copy-start(bf16[512,2048]{1,0:T(8,128)(2,1)} %weight_ref.1) | copy-start | bytes 6291460
  47.1 54.3 %copy-start.10 = (f32[2048]{0:T(1024)S(1)}, f32[2048]{0:T(1024)}, u32[]{:S(2)}) copy-start(f32[2048]{0:T(1024)} %param.14) | copy-start | bytes 24580
  53.0 1.1 copy-start.9
  57.3 10.3 %collective-permute-start.3 = (bf16[320,512]{1,0:T(8,128)(2,1)S(1)}, bf16[320,512]{1,0:T(8,128)(2,1)S(1)}, u32[]{:S(2)}, u32[]{:S(2)}) collective-permute-start(bf16[320,512]{1,0:T(8,128)(2,1)S(1)} %get-tuple-element.25), channel_id=1, source_target_pairs={{0,1},{1,2},{2,3},{3,0},{4,5},{5,6},{6,7},{7,4},{8,9},{9,10},{10,1... | collective-permute-start | bytes 983048 | tf_op jit(solution)/shard_map/ppermute | solution.py:33
  57.4 10.4 %collective-permute-start.6 = (bf16[320,512]{1,0:T(8,128)(2,1)S(1)}, bf16[320,512]{1,0:T(8,128)(2,1)S(1)}, u32[]{:S(2)}, u32[]{:S(2)}) collective-permute-start(bf16[320,512]{1,0:T(8,128)(2,1)S(1)} %get-tuple-element.28), channel_id=1, source_target_pairs={{0,3},{1,0},{2,1},{3,2},{4,7},{5,4},{6,5},{7,6},{8,11},{9,8},{10,9... | collective-permute-start | bytes 983048 | tf_op jit(solution)/shard_map/ppermute | solution.py:33
  60.1 13.6 %collective-permute-start.2 = (bf16[320,512]{1,0:T(8,128)(2,1)S(1)}, bf16[320,512]{1,0:T(8,128)(2,1)S(1)}, u32[]{:S(2)}, u32[]{:S(2)}) collective-permute-start(bf16[320,512]{1,0:T(8,128)(2,1)S(1)} %get-tuple-element.23), channel_id=1, source_target_pairs={{0,3},{1,0},{2,1},{3,2},{4,7},{5,4},{6,5},{7,6},{8,11},{9,8},{10,9... | collective-permute-start | bytes 983048 | tf_op jit(solution)/shard_map/ppermute | solution.py:33
  60.1 14.5 %collective-permute-start.5 = (bf16[320,512]{1,0:T(8,128)(2,1)S(1)}, bf16[320,512]{1,0:T(8,128)(2,1)S(1)}, u32[]{:S(2)}, u32[]{:S(2)}) collective-permute-start(bf16[320,512]{1,0:T(8,128)(2,1)S(1)} %get-tuple-element.26), channel_id=1, source_target_pairs={{0,1},{1,2},{2,3},{3,0},{4,5},{5,6},{6,7},{7,4},{8,9},{9,10},{10,1... | collective-permute-start | bytes 983048 | tf_op jit(solution)/shard_map/ppermute | solution.py:33
  67.7 14.0 %collective-permute-start.4 = (bf16[320,512]{1,0:T(8,128)(2,1)S(1)}, bf16[320,512]{1,0:T(8,128)(2,1)S(1)}, u32[]{:S(2)}, u32[]{:S(2)}) collective-permute-start(bf16[320,512]{1,0:T(8,128)(2,1)S(1)} %add_convert_fusion.2), channel_id=1, source_target_pairs={{0,1},{1,2},{2,3},{3,0},{4,5},{5,6},{6,7},{7,4},{8,9},{9,10},{10,1... | collective-permute-start | bytes 983048 | tf_op jit(solution)/shard_map/ppermute | solution.py:33
  67.9 13.7 %collective-permute-start.7 = (bf16[320,512]{1,0:T(8,128)(2,1)S(1)}, bf16[320,512]{1,0:T(8,128)(2,1)S(1)}, u32[]{:S(2)}, u32[]{:S(2)}) collective-permute-start(bf16[320,512]{1,0:T(8,128)(2,1)S(1)} %add_convert_fusion.1), channel_id=1, source_target_pairs={{0,3},{1,0},{2,1},{3,2},{4,7},{5,4},{6,5},{7,6},{8,11},{9,8},{10,9... | collective-permute-start | bytes 983048 | tf_op jit(solution)/shard_map/ppermute | solution.py:33
  81.8 15.3 %collective-permute-start.9 = (bf16[640,512]{1,0:T(8,128)(2,1)S(1)}, bf16[640,512]{1,0:T(8,128)(2,1)S(1)}, u32[]{:S(2)}, u32[]{:S(2)}) collective-permute-start(bf16[640,512]{1,0:T(8,128)(2,1)S(1)} %settle.1.own_ref.base_ref), channel_id=1, source_target_pairs={{0,3},{1,0},{2,1},{3,2},{4,7},{5,4},{6,5},{7,6},{8,11},{9,8},{10,9... | collective-permute-start | bytes 1966088 | tf_op jit(solution)/shard_map/ppermute | solution.py:33
  84.3 16.3 %collective-permute-start.8 = (bf16[640,512]{1,0:T(8,128)(2,1)S(1)}, bf16[640,512]{1,0:T(8,128)(2,1)S(1)}, u32[]{:S(2)}, u32[]{:S(2)}) collective-permute-start(bf16[640,512]{1,0:T(8,128)(2,1)S(1)} %settle.1.own_ref.base_ref), channel_id=1, source_target_pairs={{0,1},{1,2},{2,3},{3,0},{4,5},{5,6},{6,7},{7,4},{8,9},{9,10},{10,1... | collective-permute-start | bytes 1966088 | tf_op jit(solution)/shard_map/ppermute | solution.py:33
  97.2 3.5 %copy-start = (bf16[640,512]{1,0:T(8,128)(2,1)}, bf16[640,512]{1,0:T(8,128)(2,1)S(1)}, u32[]{:S(2)}) copy-start(bf16[640,512]{1,0:T(8,128)(2,1)S(1)} %collective-permute-done.9.right_ref) | copy-start | bytes 1966084
  97.2 8.3 %collective-permute-start.11 = (bf16[320,512]{1,0:T(8,128)(2,1)S(1)}, bf16[320,512]{1,0:T(8,128)(2,1)S(1)}, u32[]{:S(2)}, u32[]{:S(2)}) collective-permute-start(bf16[320,512]{1,0:T(8,128)(2,1)S(1)} %slice.114), channel_id=1, source_target_pairs={{0,3},{1,0},{2,1},{3,2},{4,7},{5,4},{6,5},{7,6},{8,11},{9,8},{10,9... | collective-permute-start | bytes 983048 | tf_op jit(solution)/shard_map/ppermute | solution.py:33
  101.5 8.1 %collective-permute-start.10 = (bf16[320,512]{1,0:T(8,128)(2,1)S(1)}, bf16[320,512]{1,0:T(8,128)(2,1)S(1)}, u32[]{:S(2)}, u32[]{:S(2)}) collective-permute-start(bf16[320,512]{1,0:T(8,128)(2,1)S(1)} %slice.113), channel_id=1, source_target_pairs={{0,1},{1,2},{2,3},{3,0},{4,5},{5,6},{6,7},{7,4},{8,9},{9,10},{10,1... | collective-permute-start | bytes 983048 | tf_op jit(solution)/shard_map/ppermute | solution.py:33
  111.4 1.1 copy-start.3
  141.1 11.7 %collective-permute-start.13 = (bf16[352,512]{1,0:T(8,128)(2,1)S(1)}, bf16[352,512]{1,0:T(8,128)(2,1)S(1)}, u32[]{:S(2)}, u32[]{:S(2)}) collective-permute-start(bf16[352,512]{1,0:T(8,128)(2,1)S(1)} %get-tuple-element.35), channel_id=1, source_target_pairs={{0,1},{1,2},{2,3},{3,0},{4,5},{5,6},{6,7},{7,4},{8,9},{9,10},{10,1... | collective-permute-start | bytes 1081352 | tf_op jit(solution)/shard_map/ppermute | solution.py:33
  148.6 13.1 %collective-permute-start.15 = (bf16[288,512]{1,0:T(8,128)(2,1)S(1)}, bf16[288,512]{1,0:T(8,128)(2,1)S(1)}, u32[]{:S(2)}, u32[]{:S(2)}) collective-permute-start(bf16[288,512]{1,0:T(8,128)(2,1)S(1)} %get-tuple-element.36), channel_id=1, source_target_pairs={{0,1},{1,2},{2,3},{3,0},{4,5},{5,6},{6,7},{7,4},{8,9},{9,10},{10,1... | collective-permute-start | bytes 884744 | tf_op jit(solution)/shard_map/ppermute | solution.py:33
  149.9 7.7 %collective-permute-start.16 = (bf16[288,512]{1,0:T(8,128)(2,1)S(1)}, bf16[288,512]{1,0:T(8,128)(2,1)S(1)}, u32[]{:S(2)}, u32[]{:S(2)}) collective-permute-start(bf16[288,512]{1,0:T(8,128)(2,1)S(1)} %get-tuple-element.38), channel_id=1, source_target_pairs={{0,3},{1,0},{2,1},{3,2},{4,7},{5,4},{6,5},{7,6},{8,11},{9,8},{10,9... | collective-permute-start | bytes 884744 | tf_op jit(solution)/shard_map/ppermute | solution.py:33
  151.3 14.0 %collective-permute-start.12 = (bf16[352,512]{1,0:T(8,128)(2,1)S(1)}, bf16[352,512]{1,0:T(8,128)(2,1)S(1)}, u32[]{:S(2)}, u32[]{:S(2)}) collective-permute-start(bf16[352,512]{1,0:T(8,128)(2,1)S(1)} %get-tuple-element.33), channel_id=1, source_target_pairs={{0,3},{1,0},{2,1},{3,2},{4,7},{5,4},{6,5},{7,6},{8,11},{9,8},{10,9... | collective-permute-start | bytes 1081352 | tf_op jit(solution)/shard_map/ppermute | solution.py:33
  153.0 18.7 %collective-permute-start.14 = (bf16[352,512]{1,0:T(8,128)(2,1)S(1)}, bf16[352,512]{1,0:T(8,128)(2,1)S(1)}, u32[]{:S(2)}, u32[]{:S(2)}) collective-permute-start(bf16[352,512]{1,0:T(8,128)(2,1)S(1)} %add_convert_fusion), channel_id=1, source_target_pairs={{0,1},{1,2},{2,3},{3,0},{4,5},{5,6},{6,7},{7,4},{8,9},{9,10},{10,1... | collective-permute-start | bytes 1081352 | tf_op jit(solution)/shard_map/ppermute | solution.py:33
  157.7 14.0 %collective-permute-start.17 = (bf16[288,512]{1,0:T(8,128)(2,1)S(1)}, bf16[288,512]{1,0:T(8,128)(2,1)S(1)}, u32[]{:S(2)}, u32[]{:S(2)}) collective-permute-start(bf16[288,512]{1,0:T(8,128)(2,1)S(1)} %add_convert_fusion.3), channel_id=1, source_target_pairs={{0,3},{1,0},{2,1},{3,2},{4,7},{5,4},{6,5},{7,6},{8,11},{9,8},{10,9... | collective-permute-start | bytes 884744 | tf_op jit(solution)/shard_map/ppermute | solution.py:33
  (6 other events, 5.4 us)
Sparse Core Ops, SparseCore 0:
  9.2 122.4 all-gather.1
